TPU v7x, 32 devices: a whole 2x2x4 slice. The times are simulated.
32 devices in a mesh: ep: 8 (over z, y), tp: 4 (over x, core).
Axes of the slice: x: 2, y: 2, z: 4, core: 2. Of those that a mesh axis runs over, the one named last changes fastest.
Arguments:
- queries: bfloat16 [4096, 1024], P('ep', 'tp'), may hold values from -6 to 6
- keys: bfloat16 [4096, 512], P('ep', 'tp'), may hold values from -6 to 6
- values: bfloat16 [4096, 512], P('ep', 'tp'), may hold values from -6 to 6
- forget_cache: float32 [8, 4096], P('tp'), may hold values from -412 to 0, as said below
- query_gain: float32 [128], replicated, may hold values from 0.6 to 6
- key_gain: float32 [128], replicated, may hold values from 0.6 to 6
- mixer_out: bfloat16 [1024, 2048], replicated, may hold values from -0.75 to 0.75
- expert_input: bfloat16 [4096, 2048], P(('ep', 'tp')), may hold values from -6 to 6
- norm_gain: float32 [2048], replicated, may hold values from 0.1 to 1.9
- routes: int32 [4096, 2], P(('ep', 'tp')), may hold values from 0 to 31, all different within a row; in each aligned block of 128 rows (0 to 127, 128 to 255, ...) at most 16 rows name the same one
- route_weights: float32 [4096, 2], P(('ep', 'tp')), may hold values from 0.1 to 1
- w_gate: bfloat16 [32, 2048, 1024], P('ep', None, 'tp'), may hold values from -0.125 to 0.125
- w_up: bfloat16 [32, 2048, 1024], P('ep', None, 'tp'), may hold values from -0.125 to 0.125
- w_down: bfloat16 [32, 2048, 1024], P('ep', None, 'tp'), may hold values from -0.1875 to 0.1875
Outputs:
- mixed: bfloat16 [4096, 2048], P(('ep', 'tp'))
- routed: bfloat16 [4096, 2048], P(('ep', 'tp'))
Inputs may be any that keep to these rules, and one draw needn't show every extreme that they name: `routes`: each row names 2 different experts; among the rows of one device no expert is named by more than 16 rows, a bound that some block reaches. `forget_cache`: never rises along the positions.
All inputs are finite; a program needn't handle non-finite values.
Results may differ from a plain program's by a relative error of at most 0.013.
The roundings to bfloat16 on the way count: a program that leaves them out, or rounds other values in their place, can miss the bound.
Values may be sent and summed in bfloat16 or wider, within the bound.
A program may use at most 128 MiB of HBM per device.

v0:
```python
import functools

import jax
import jax.numpy as jnp
from jax import lax
from jax.experimental import pallas as pl
from jax.experimental.pallas import tpu as pltpu
from jax.sharding import PartitionSpec as P

CAP = 16
EPSILON = 1e-06
NEGATIVE = -1e30
MESH = pl.DeviceIdType.MESH
VMEM_LIMIT = 62 * 1024 * 1024


def rms_scale(inputs, gain):
    inputs = inputs.astype(jnp.float32)
    return inputs * lax.rsqrt(jnp.mean(inputs * inputs, axis=-1, keepdims=True) + EPSILON) * gain


def places(n_tp):
    ep, tp = lax.axis_index("ep"), lax.axis_index("tp")
    core = tp + 1 - 2 * lax.rem(tp, 2)
    across = lax.rem(tp + n_tp // 2, n_tp)
    corner = lax.rem(core + n_tp // 2, n_tp)
    return ep, tp, core, across, corner


def weights_of(count):
    digits = count.bit_length() - 1
    assert count == 1 << digits
    return [1] + [1 << (digits - number) for number in range(1, digits)]


def paired(place, slot, count):
    result = 0
    for number, weight in enumerate(weights_of(count)):
        result = result + weight * lax.rem(lax.div(place, weight) + lax.div(slot, 1 << number), 2)
    return result


def meet(n_ep, n_tp):
    ep, tp = lax.axis_index("ep"), lax.axis_index("tp")
    barrier = pltpu.get_barrier_semaphore()
    for step in range(1, n_ep):
        pl.semaphore_signal(
            barrier, inc=1, device_id=(lax.rem(ep + step, n_ep), tp), device_id_type=MESH
        )
    for step in range(1, n_tp):
        pl.semaphore_signal(
            barrier, inc=1, device_id=(ep, lax.rem(tp + step, n_tp)), device_id_type=MESH
        )
    pl.semaphore_wait(barrier, n_ep + n_tp - 2)


def remote(src, dst, send, recv, ep, tp):
    return pltpu.make_async_remote_copy(
        src_ref=src, dst_ref=dst, send_sem=send, recv_sem=recv, device_id=(ep, tp), device_id_type=MESH
    )


def layer_kernel(
    n_ep,
    n_tp,
    heads,
    outg,
    kv,
    q,
    fq,
    fk,
    slots_weights,
    gate_hbm,
    up_hbm,
    down_hbm,
    mixer_hbm,
    mixed,
    routed,
    gate_w,
    up_w,
    down_w,
    mixer,
    kvbuf,
    att,
    att_all,
    high,
    denom,
    accum,
    pieces,
    sums,
    near_own,
    near_far,
    sum_x,
    got_x,
    sum_r,
    back,
    a_send,
    a_recv,
    x_send,
    x_recv,
    c_send,
    c_recv,
    d_send,
    d_recv,
    u_send,
    k_send,
    k_recv,
    f_send,
    f_recv,
    n_send,
    n_recv,
    y_send,
    y_recv,
    r_send,
    r_recv,
    t_send,
    t_recv,
    w_sem,
    own_sem,
):
    ep, tp, core, across, corner = places(n_tp)
    rows, head_dim = kv.shape[0], q.shape[1]
    part = rows // n_tp
    scale = head_dim ** (-0.5)
    local, width, ff = gate_w.shape
    half = n_ep // 2
    level, side = lax.div(ep, 2), lax.rem(ep, 2)
    levels = n_ep // 2
    beside = ep + 1 - 2 * side
    assert local <= half
    loads = [
        pltpu.make_async_copy(src, dst, w_sem.at[number])
        for number, (src, dst) in enumerate(
            [(gate_hbm, gate_w), (up_hbm, up_w), (down_hbm, down_w), (mixer_hbm, mixer)]
        )
    ]
    meet(n_ep, n_tp)

    def up_copy(src, source):
        above = lax.rem(ep + 2, n_ep)
        return remote(src, kvbuf.at[source], u_send.at[source], k_recv.at[source], above, tp)

    def side_copy(src, source):
        return remote(src, kvbuf.at[source], k_send.at[source], k_recv.at[source], beside, tp)

    def a_copy(slot):
        other = paired(ep, slot, n_ep)
        return remote(outg.at[slot], pieces.at[tp, slot], a_send.at[slot], a_recv.at[slot], other, tp)

    def x_copy(src, owner, slot):
        return remote(src, pieces.at[owner, slot], x_send.at[slot], x_recv.at[slot], ep, across)

    def c_copy(src, owner, slot):
        return remote(src, pieces.at[owner, slot], c_send.at[slot], c_recv.at[slot], ep, core)

    def d_copy(src, owner, slot):
        return remote(src, pieces.at[owner, slot], d_send.at[slot], d_recv.at[slot], ep, core)

    def far_copy(slot):
        return remote(sums.at[corner, slot], near_far.at[slot], f_send.at[slot], f_recv.at[slot], ep, core)

    def own_copy(slot):
        return remote(sums.at[core, slot], near_own.at[slot], n_send.at[slot], n_recv.at[slot], ep, core)

    def y_copy(slot):
        return remote(sum_x.at[slot], got_x.at[slot], y_send.at[slot], y_recv.at[slot], ep, across)

    def r_copy(slot):
        other = paired(ep, slot, n_ep)
        return remote(sum_r.at[slot], back.at[slot], r_send.at[slot], r_recv.at[slot], other, tp)

    def each(first, last, act):
        def body(number, carry):
            act(number)
            return carry

        lax.fori_loop(first, last, body, 0)

    @pl.when(level + 1 < levels)
    def _():
        up_copy(kv, ep).start()

    @pl.when(side == 0)
    def _():
        side_copy(kv, ep).start()

    own = pltpu.make_async_copy(outg.at[0], pieces.at[tp, 0], own_sem)
    own.start()
    x_copy(outg.at[0], tp, 0).start()
    c_copy(outg.at[0], tp, 0).start()
    a_copy(1).start()
    for load in loads:
        load.start()
    tile = rows // 2

    def block(source, keys_ref, diagonal):
        keys = keys_ref[:, :head_dim]
        vals = keys_ref[:, head_dim:]
        for head in range(heads):
            key_gate = fk[source, head : head + 1, :]
            for piece in range(2):
                span = pl.ds(head * rows + piece * tile, tile)
                scores = lax.dot_general(
                    q[span, :], keys, (((1,), (1,)), ((), ())), preferred_element_type=jnp.float32
                )
                scores = scores * scale + fq[span, :] - key_gate
                if diagonal:
                    qpos = piece * tile + lax.broadcasted_iota(jnp.int32, scores.shape, 0)
                    kpos = lax.broadcasted_iota(jnp.int32, scores.shape, 1)
                    scores = jnp.where(kpos <= qpos, scores, NEGATIVE)
                top = jnp.max(scores, axis=1, keepdims=True)
                if diagonal:
                    newest = top
                else:
                    before = high[span, :]
                    newest = jnp.maximum(before, top)
                weights = jnp.exp(scores - newest)
                total = jnp.sum(weights, axis=1, keepdims=True)
                product = jnp.dot(
                    weights.astype(jnp.bfloat16), vals, preferred_element_type=jnp.float32
                )
                if not diagonal:
                    factor = jnp.exp(before - newest)
                    total = denom[span, :] * factor + total
                    product = accum[span, :] * factor + product
                high[span, :] = newest
                denom[span, :] = total
                accum[span, :] = product

    def spread(source):
        side_copy(kvbuf.at[source], source).start()

        @pl.when(level + 1 < levels)
        def _():
            up_copy(kvbuf.at[source], source).start()

    def relay(slot):
        x_copy(outg.at[0], across, slot).wait_recv()
        d_copy(pieces.at[across, slot], across, slot).start()

    @pl.when(level > 0)
    def _():
        side_copy(kv, ep - 2).wait_recv()
        spread(ep - 2)

    each(2, n_ep, lambda slot: a_copy(slot).start())
    block(ep, kv, True)

    @pl.when(side == 1)
    def _():
        side_copy(kv, ep - 1).wait_recv()
        block(ep - 1, kvbuf.at[ep - 1], False)

    def landed(slot):
        c_copy(outg.at[0], core, slot).wait_recv()
        d_copy(outg.at[0], corner, slot).wait_recv()

    def expert(number, begin):
        own_rows = pl.ds(pl.multiple_of(number * CAP, CAP), CAP)
        taken = pieces[:, begin : begin + half, own_rows, :].reshape(n_tp * half * CAP, width)
        gate = jnp.dot(taken, gate_w[number], preferred_element_type=jnp.float32)
        upward = jnp.dot(taken, up_w[number], preferred_element_type=jnp.float32)
        hidden = (gate / (1.0 + jnp.exp(-gate)) * upward).astype(jnp.bfloat16)
        columns = min(width, 512)
        for begin_column in range(0, width, columns):
            lanes = slice(begin_column, begin_column + columns)
            result = lax.dot_general(
                hidden,
                down_w[number, lanes, :],
                (((1,), (1,)), ((), ())),
                preferred_element_type=jnp.float32,
            )
            sums[:, begin : begin + half, own_rows, lanes] = result.astype(jnp.bfloat16).reshape(
                n_tp, half, CAP, columns
            )

    def onward(slot):
        a_copy(slot).wait_recv()
        x_copy(pieces.at[tp, slot], tp, slot).start()
        c_copy(pieces.at[tp, slot], tp, slot).start()

        below = level - lax.div(slot + 1, 2)
        turned = lax.rem(slot + 1, 2)
        lower = 2 * below + lax.rem(side + turned, 2)

        @pl.when(below >= 0)
        def _():
            @pl.when(slot > 1)
            def _():
                side_copy(kv, lower).wait_recv()

                @pl.when(turned == 0)
                def _():
                    spread(lower)

            block(lower, kvbuf.at[lower], False)

        relay(slot - 1)

    each(1, half, onward)

    def onward_and_expert(slot):
        onward(slot)

        @pl.when(slot == half)
        def _():
            own.wait()
            for load in loads:
                load.wait()
            each(0, half, landed)

        @pl.when(slot - half < local)
        def _():
            expert(slot - half, 0)

    each(half, n_ep, onward_and_expert)
    relay(n_ep - 1)

    def hand_over(begin):
        each(0, half, lambda step: far_copy(begin + half - 1 - step).start())
        each(0, half, lambda step: own_copy(begin + half - 1 - step).start())

        def add(step):
            slot = begin + half - 1 - step
            far_copy(slot).wait_recv()
            sum_x[slot] = (
                sums[across, slot].astype(jnp.float32) + near_far[slot].astype(jnp.float32)
            ).astype(jnp.bfloat16)
            y_copy(slot).start()

        each(0, half, add)

    def total_of(slot):
        own_copy(slot).wait_recv()
        y_copy(slot).wait_recv()
        return (
            sums[tp, slot].astype(jnp.float32)
            + near_own[slot].astype(jnp.float32)
            + got_x[slot].astype(jnp.float32)
        ).astype(jnp.bfloat16)

    def send_back(slot):
        sum_r[slot] = total_of(slot)
        r_copy(slot).start()

    hand_over(0)
    for head in range(heads):
        span = pl.ds(head * rows, rows)
        result = (accum[span, :] / denom[span, :]).astype(jnp.bfloat16)
        for owner in range(n_tp):
            att[owner, head] = result[owner * part : (owner + 1) * part]

    def t_copy(source, step):
        dest = lax.rem(tp + step, n_tp)
        return remote(att.at[dest], att_all.at[source], t_send.at[step], t_recv.at[source], ep, dest)

    for step in range(1, n_tp):
        t_copy(tp, step).start()
    att_all[tp] = att[tp]

    each(half, n_ep, landed)
    each(0, local, lambda number: expert(number, half))
    hand_over(half)

    each(1, half, lambda step: send_back(half - step))
    back[0] = total_of(0)

    for step in range(1, n_tp):
        t_copy(lax.rem(tp - step + n_tp, n_tp), step).wait()
    total = None
    for source in range(n_tp):
        for head in range(heads):
            number = source * heads + head
            term = jnp.dot(
                att_all[source, head],
                mixer[number * head_dim : (number + 1) * head_dim, :],
                preferred_element_type=jnp.float32,
            )
            total = term if total is None else total + term
    mixed[...] = total.astype(jnp.bfloat16)

    each(0, half, lambda step: send_back(n_ep - 1 - step))

    def sent(slot):
        x_copy(outg.at[0], tp, slot).wait_send()
        c_copy(outg.at[0], tp, slot).wait_send()
        d_copy(outg.at[0], tp, slot).wait_send()
        far_copy(slot).wait_send()
        own_copy(slot).wait_send()
        y_copy(slot).wait_send()

    each(0, n_ep, sent)
    each(1, n_ep, lambda slot: a_copy(slot).wait_send())

    @pl.when(level + 1 < levels)
    def _():
        up_copy(kv, ep).wait_send()

    @pl.when(side == 0)
    def _():
        side_copy(kv, ep).wait_send()

    def spread_sent(k):
        source = ep - 2 * k
        side_copy(kv, source).wait_send()

        @pl.when(level + 1 < levels)
        def _():
            up_copy(kv, source).wait_send()

    each(1, level + 1, spread_sent)
    each(1, n_ep, lambda slot: r_copy(slot).wait())

    _, per, _ = back.shape
    found_rows = back[...].reshape(n_ep * per, width)
    summed = None
    top = slots_weights.shape[1] // 2
    for choice in range(top):
        lanes = lax.broadcasted_iota(jnp.int32, (mixed.shape[0], n_ep * per), 1)
        pick = jnp.where(
            lanes.astype(jnp.float32) == slots_weights[:, choice : choice + 1], 1.0, 0.0
        ).astype(jnp.bfloat16)
        found = jnp.dot(pick, found_rows, preferred_element_type=jnp.float32)
        term = found * slots_weights[:, top + choice : top + choice + 1]
        summed = term if summed is None else summed + term
    routed[...] = summed.astype(jnp.bfloat16)


def on_device(
    n_ep,
    n_tp,
    queries,
    keys,
    values,
    forget_cache,
    query_gain,
    key_gain,
    mixer_out,
    expert_input,
    norm_gain,
    routes,
    route_weights,
    w_gate,
    w_up,
    w_down,
):
    rows, head_dim = keys.shape
    heads = forget_cache.shape[0]
    ep = lax.axis_index("ep")
    local, width, ff = w_gate.shape
    experts = local * n_ep
    tokens = expert_input.shape[0]
    per = local * CAP
    part = rows // n_tp
    vmem = pl.BlockSpec(memory_space=pltpu.VMEM)
    anywhere = pl.BlockSpec(memory_space=pl.ANY)
    dma = pltpu.SemaphoreType.DMA

    normed_q = rms_scale(queries.reshape(rows, heads, head_dim), query_gain).astype(jnp.bfloat16)
    q = normed_q.transpose(1, 0, 2).reshape(heads * rows, head_dim)
    kv = jnp.concatenate([rms_scale(keys, key_gain).astype(jnp.bfloat16), values], axis=1)
    fq = lax.dynamic_slice_in_dim(forget_cache, ep * rows, rows, 1).reshape(heads * rows, 1)
    fk = forget_cache.reshape(heads, n_ep, rows).transpose(1, 0, 2)

    normed = rms_scale(expert_input, norm_gain).astype(jnp.bfloat16)
    names = jnp.arange(experts, dtype=jnp.int32)
    named = [(routes[:, k : k + 1] == names[None, :]) for k in range(routes.shape[1])]
    anyone = functools.reduce(jnp.logical_or, named).astype(jnp.bfloat16)
    at = jnp.arange(tokens, dtype=jnp.int32)
    earlier = (at[None, :] < at[:, None]).astype(jnp.bfloat16)
    prior = jnp.dot(earlier, anyone, preferred_element_type=jnp.float32)
    ranks = [jnp.sum(jnp.where(mine, prior, 0.0), axis=1).astype(jnp.int32) for mine in named]
    differ = (routes // local) ^ ep
    slot = jnp.zeros_like(routes)
    for number, weight in enumerate(weights_of(n_ep)):
        slot = slot + (1 << number) * (differ // weight % 2)
    base = slot * per + routes % local * CAP
    slots = jnp.stack([base[:, k] + rank for k, rank in enumerate(ranks)], axis=1)
    slots_weights = jnp.concatenate([slots.astype(jnp.float32), route_weights], axis=1)
    line = jnp.arange(experts * CAP, dtype=jnp.int32)[:, None]
    place = functools.reduce(
        jnp.logical_or, [line == slots[:, k][None, :] for k in range(slots.shape[1])]
    ).astype(jnp.bfloat16)
    outg = jnp.dot(place, normed, preferred_element_type=jnp.float32).astype(jnp.bfloat16)
    outg = outg.reshape(n_ep, per, width)

    buffer = pltpu.VMEM((n_ep, per, width), jnp.bfloat16)
    return pl.pallas_call(
        functools.partial(layer_kernel, n_ep, n_tp, heads),
        out_shape=(
            jax.ShapeDtypeStruct((part, width), jnp.bfloat16),
            jax.ShapeDtypeStruct((tokens, width), jnp.bfloat16),
        ),
        in_specs=[vmem] * 6 + [anywhere] * 4,
        out_specs=(vmem, vmem),
        scratch_shapes=[pltpu.VMEM(w_gate.shape, jnp.bfloat16)] * 3
        + [
            pltpu.VMEM(mixer_out.shape, jnp.bfloat16),
            pltpu.VMEM((n_ep, rows, 2 * head_dim), jnp.bfloat16),
            pltpu.VMEM((n_tp, heads, part, head_dim), jnp.bfloat16),
            pltpu.VMEM((n_tp, heads, part, head_dim), jnp.bfloat16),
            pltpu.VMEM((heads * rows, 1), jnp.float32),
            pltpu.VMEM((heads * rows, 1), jnp.float32),
            pltpu.VMEM((heads * rows, head_dim), jnp.float32),
            pltpu.VMEM((n_tp, n_ep, per, width), jnp.bfloat16),
            pltpu.VMEM((n_tp, n_ep, per, width), jnp.bfloat16),
        ]
        + [buffer] * 6
        + [dma((n_ep,))] * 19
        + [dma((n_tp,))] * 3
        + [dma],
        compiler_params=pltpu.CompilerParams(
            collective_id=0, has_side_effects=True, vmem_limit_bytes=VMEM_LIMIT
        ),
        name="layer",
    )(outg, kv, q, fq, fk, slots_weights, w_gate, w_up, w_down, mixer_out)


def solution(mesh):
    n_ep, n_tp = mesh.shape["ep"], mesh.shape["tp"]
    in_specs = (
        P("ep", "tp"),
        P("ep", "tp"),
        P("ep", "tp"),
        P("tp", None),
        P(),
        P(),
        P(),
        P(("ep", "tp"), None),
        P(),
        P(("ep", "tp"), None),
        P(("ep", "tp"), None),
        P("ep", None, "tp"),
        P("ep", None, "tp"),
        P("ep", None, "tp"),
    )
    out_specs = (P(("ep", "tp"), None), P(("ep", "tp"), None))
    return jax.shard_map(
        functools.partial(on_device, n_ep, n_tp),
        mesh=mesh,
        in_specs=in_specs,
        out_specs=out_specs,
        check_vma=False,
    )
```

profile of v0, /device:TPU:22, one launch (start us, length us, event | category | flops | bytes accessed | tf_op | source)
XLA Modules:
  0.0 163.3 jit_solution(1297141234089240246)
XLA Ops:
  0.6 0.0 copy-start
  0.6 0.0 copy-start.1
  0.7 0.0 copy-start.2
  0.7 0.8 fusion.24
  1.4 1.2 fusion
  2.7 0.8 slice_bitcast_fusion.1
  3.4 0.2 select_reduce_fusion.1
  3.6 0.7 pad_maximum_fusion.1
  4.3 1.0 fusion.6
  5.4 0.7 dynamic-slice_bitcast_fusion
  6.1 0.7 copy.46.slots_weights
  6.8 1.0 fusion.8
  7.9 1.6 %pad_maximum_fusion.kv = bf16[512,256]{1,0:T(8,128)(2,1)} fusion(bf16[512,128]{1,0:T(8,128)(2,1)} %param.16, bf16[512,128]{1,0:T(8,128)(2,1)S(1)} %fusion.8), kind=kLoop, calls=%fused_computation.17 | loop fusion | flops 524288 | bytes 524288 | tf_op jit(solution)/shard_map/concatenate | solution.py:461
  9.5 1.0 copy.48
  10.5 1.2 reshape.82
  11.7 0.6 multiply_reduce_fusion
  12.4 0.0 copy-done.2
  12.4 0.7 fusion.9
  13.2 0.8 copy.44
  13.9 0.0 copy-done
  13.9 0.0 copy-done.1
  13.9 2.1 %convolution_convert_fusion = bf16[512,2048]{1,0:T(8,128)(2,1)} fusion(bf16[128,2048]{1,0:T(8,128)(2,1)S(1)} %copy-done, f32[2048]{0:T(1024)S(1)} %copy-done.1, f32[128]{0:T(128)S(1)} %add_rsqrt_fusion.2, s32[128]{0:T(128)S(1)} %get-tuple-element.7, s32[128]{0:T(128)S(1)} %get-tuple-element.6), kind=kOutput, calls=%fused_computation | convolution fusion | flops 270729216 | bytes 2631168 | tf_op jit(solution)/shard_map/dot_general | solution.py:484
  16.1 143.5 %layer.1 = (bf16[128,2048]{1,0:T(8,128)(2,1)}, bf16[128,2048]{1,0:T(8,128)(2,1)}) custom-call(bf16[8,64,2048]{2,1,0:T(8,128)(2,1)} %bitcast.24, bf16[512,256]{1,0:T(8,128)(2,1)} %pad_maximum_fusion.kv, bf16[1024,128]{1,0:T(8,128)(2,1)} %bitcast.26, f32[1024,1]{1,0:T(8,128)} %bitcast.25, f32[8,2,512]{2,1,0:T(2,128)} %bitcast.27, ...), custom_call_target="tpu_custom_call" | custom-call | tf_op jit(solution)/shard_map/layer/pallas_call | solution.py:488
  159.6 1.9 %copy.52 = bf16[128,2048]{1,0:T(8,128)(2,1)} copy(bf16[128,2048]{1,0:T(8,128)(2,1)} %get-tuple-element.12) | data formatting | bytes 1048576
  161.4 1.9 %copy.53 = bf16[128,2048]{1,0:T(8,128)(2,1)} copy(bf16[128,2048]{1,0:T(8,128)(2,1)} %get-tuple-element.13) | data formatting | bytes 1048576
  (7 shorter events, 0.1 us)
Async XLA Ops:
  0.6 13.3 %copy-start = (bf16[128,2048]{1,0:T(8,128)(2,1)S(1)}, bf16[128,2048]{1,0:T(8,128)(2,1)}, u32[]{:S(2)}) copy-start(bf16[128,2048]{1,0:T(8,128)(2,1)} %param.21) | copy-start | bytes 1572868
  0.6 13.3 %copy-start.1 = (f32[2048]{0:T(1024)S(1)}, f32[2048]{0:T(1024)}, u32[]{:S(2)}) copy-start(f32[2048]{0:T(1024)} %param.22) | copy-start | bytes 24580
  0.7 11.8 %copy-start.2 = (f32[128]{0:T(128)S(1)}, f32[128]{0:T(128)}, u32[]{:S(2)}) copy-start(f32[128]{0:T(128)} %param.18) | copy-start | bytes 1540
where the time goes:
time: 164 us; the launch traced here: 163 us
  Pallas kernels  144 us (88%)
  local copies, waits for them, and re-layouts  8.96 us (5%)
  other arithmetic  7.83 us (5%)
  matrix products  2.29 us (1%)
    pallas_call x1, Pallas kernels, on_device(): pl.pallas_call(functools.partial(layer_kernel, n_ep, n_tp, heads), out_sh...  144 us
    unnamed x11, local copies, waits for them, and re-layouts  5.5 us

commit v1 on v0

v1 whole, which is shorter than its diff:
```python
import functools

import jax
import jax.numpy as jnp
from jax import lax
from jax.experimental import pallas as pl
from jax.experimental.pallas import tpu as pltpu
from jax.sharding import PartitionSpec as P

CAP = 16
EPSILON = 1e-06
NEGATIVE = -1e30
MESH = pl.DeviceIdType.MESH
VMEM_LIMIT = 62 * 1024 * 1024


def places(n_tp):
    ep, tp = lax.axis_index("ep"), lax.axis_index("tp")
    core = tp + 1 - 2 * lax.rem(tp, 2)
    across = lax.rem(tp + n_tp // 2, n_tp)
    corner = lax.rem(core + n_tp // 2, n_tp)
    return ep, tp, core, across, corner


def remote(src, dst, send, recv, ep, tp):
    return pltpu.make_async_remote_copy(
        src_ref=src, dst_ref=dst, send_sem=send, recv_sem=recv, device_id=(ep, tp), device_id_type=MESH
    )


def normed_rows(ref, columns, gain):
    values = ref[:, columns].astype(jnp.float32)
    inverse = lax.rsqrt(jnp.mean(values * values, axis=-1, keepdims=True) + EPSILON)
    return (values * inverse * gain).astype(jnp.bfloat16)


def layer_kernel(
    n_ep,
    n_tp,
    tokens_in,
    norm_gain,
    routes,
    route_weights,
    queries,
    keys_in,
    values_in,
    forget,
    query_gain,
    key_gain,
    gate_hbm,
    up_hbm,
    down_hbm,
    mixer_hbm,
    mixed,
    routed,
    gate_w,
    up_w,
    down_w,
    mixer,
    kv,
    kvbuf,
    q,
    fq,
    tok,
    meta,
    ysend,
    att,
    att_all,
    high,
    denom,
    accum,
    pieces,
    sums,
    near_own,
    near_far,
    sum_x,
    got_x,
    sum_r,
    back,
    x_send,
    x_recv,
    c_send,
    c_recv,
    d_send,
    d_recv,
    f_send,
    f_recv,
    n_send,
    n_recv,
    y_send,
    y_recv,
    r_send,
    r_recv,
    zu_send,
    zd_send,
    z_recv,
    mu_send,
    md_send,
    m_recv,
    b_send,
    b_recv,
    u_send,
    k_send,
    k_recv,
    t_send,
    t_recv,
    w_sem,
):
    ep, tp, core, across, corner = places(n_tp)
    rows, head_dim = keys_in.shape
    heads = forget.shape[0]
    part = rows // n_tp
    scale = head_dim ** (-0.5)
    local, width, ff = gate_w.shape
    per = local * CAP
    tokens = tokens_in.shape[0]
    choices = routes.shape[0]
    level, side = lax.div(ep, 2), lax.rem(ep, 2)
    levels = n_ep // 2
    beside = ep + 1 - 2 * side
    above = lax.rem(ep + 2, n_ep)
    below = lax.rem(ep + n_ep - 2, n_ep)
    both = jnp.minimum(level, levels - 1 - level)
    assert levels >= 4

    loads = [
        pltpu.make_async_copy(src, dst, w_sem.at[number])
        for number, (src, dst) in enumerate(
            [(gate_hbm, gate_w), (up_hbm, up_w), (down_hbm, down_w), (mixer_hbm, mixer)]
        )
    ]
    for load in loads:
        load.start()

    barrier = pltpu.get_barrier_semaphore()
    for step in range(1, n_ep):
        pl.semaphore_signal(
            barrier, inc=1, device_id=(lax.rem(ep + step, n_ep), tp), device_id_type=MESH
        )
    for step in range(1, n_tp):
        pl.semaphore_signal(
            barrier, inc=1, device_id=(ep, lax.rem(tp + step, n_tp)), device_id_type=MESH
        )

    def each(first, last, act):
        def body(number, carry):
            act(number)
            return carry

        lax.fori_loop(first, last, body, 0)

    def level_of(number):
        near = lax.div(number + 1, 2)
        odd = lax.rem(number, 2)
        far = number - both
        paired = level + near * (1 - 2 * odd)
        lone = jnp.where(level < levels - 1 - level, level + far, level - far)
        return jnp.where(number <= 2 * both, paired, lone)

    def z_up(source):
        return remote(tok.at[source], tok.at[source], zu_send.at[source], z_recv.at[source], above, tp)

    def z_down(source):
        return remote(tok.at[source], tok.at[source], zd_send.at[source], z_recv.at[source], below, tp)

    def m_up(source):
        return remote(meta.at[source], meta.at[source], mu_send.at[source], m_recv.at[source], above, tp)

    def m_down(source):
        return remote(meta.at[source], meta.at[source], md_send.at[source], m_recv.at[source], below, tp)

    def b_copy(number):
        slot = 2 * number + side
        return remote(
            ysend.at[number], pieces.at[tp, slot], b_send.at[number], b_recv.at[number], beside, tp
        )

    def up_copy(src, source):
        return remote(src, kvbuf.at[source], u_send.at[source], k_recv.at[source], above, tp)

    def side_copy(src, source):
        return remote(src, kvbuf.at[source], k_send.at[source], k_recv.at[source], beside, tp)

    def x_copy(slot):
        return remote(
            pieces.at[tp, slot], pieces.at[tp, slot], x_send.at[slot], x_recv.at[slot], ep, across
        )

    def c_copy(slot):
        return remote(
            pieces.at[tp, slot], pieces.at[tp, slot], c_send.at[slot], c_recv.at[slot], ep, core
        )

    def d_copy(slot):
        return remote(
            pieces.at[across, slot], pieces.at[across, slot], d_send.at[slot], d_recv.at[slot], ep, core
        )

    def far_copy(slot):
        return remote(sums.at[corner, slot], near_far.at[slot], f_send.at[slot], f_recv.at[slot], ep, core)

    def own_copy(slot):
        return remote(sums.at[core, slot], near_own.at[slot], n_send.at[slot], n_recv.at[slot], ep, core)

    def y_copy(slot):
        return remote(sum_x.at[slot], got_x.at[slot], y_send.at[slot], y_recv.at[slot], ep, across)

    def r_copy(slot, dest):
        return remote(sum_r.at[slot], back.at[ep], r_send.at[slot], r_recv.at[ep], dest, tp)

    def r_arrived(source):
        return remote(sum_r.at[0], back.at[source], r_send.at[0], r_recv.at[source], beside, tp)

    def t_copy(source, step):
        dest = lax.rem(tp + step, n_tp)
        return remote(att.at[dest], att_all.at[source], t_send.at[step], t_recv.at[source], ep, dest)

    strip = min(tokens, 32)
    for begin in range(0, tokens, strip):
        lines = slice(begin, begin + strip)
        values = tokens_in[lines, :].astype(jnp.float32)
        inverse = lax.rsqrt(jnp.mean(values * values, axis=-1, keepdims=True) + EPSILON)
        tok[level, lines, :] = (values * inverse * norm_gain[...]).astype(jnp.bfloat16)
    names = lax.broadcasted_iota(jnp.int32, (n_ep * local, tokens), 0)
    named = [names == routes[k : k + 1, :] for k in range(choices)]
    anyone = sum(jnp.where(mine, 1.0, 0.0) for mine in named).astype(jnp.bfloat16)
    earlier = jnp.where(
        lax.broadcasted_iota(jnp.int32, (tokens, tokens), 0)
        < lax.broadcasted_iota(jnp.int32, (tokens, tokens), 1),
        1.0,
        0.0,
    ).astype(jnp.bfloat16)
    prior = jnp.dot(anyone, earlier, preferred_element_type=jnp.float32)
    meta[level] = jnp.zeros(meta.shape[1:], jnp.float32)
    for k in range(choices):
        rank = jnp.sum(jnp.where(named[k], prior, 0.0), axis=0, keepdims=True)
        meta[level, k : k + 1, :] = routes[k : k + 1, :].astype(jnp.float32) * CAP + rank

    pl.semaphore_wait(barrier, n_ep + n_tp - 2)

    @pl.when(level + 1 < levels)
    def _():
        m_up(level).start()
        z_up(level).start()

    @pl.when(level > 0)
    def _():
        m_down(level).start()
        z_down(level).start()

    def select(source, place):
        lines = place * per + lax.broadcasted_iota(jnp.int32, (per, tokens), 0)
        lines = lines.astype(jnp.float32)
        picks = functools.reduce(
            jnp.logical_or, [lines == meta[source, k : k + 1, :] for k in range(choices)]
        )
        picks = jnp.where(picks, 1.0, 0.0).astype(jnp.bfloat16)
        return jnp.dot(picks, tok[source], preferred_element_type=jnp.float32).astype(jnp.bfloat16)

    def hand_out(source, number):
        slot = 2 * number + side
        pieces[tp, slot] = select(source, ep)
        x_copy(slot).start()
        c_copy(slot).start()
        ysend[number] = select(source, beside)
        b_copy(number).start()

    def from_side(number):
        slot = 2 * number + 1 - side
        b_copy(number).wait_recv()
        x_copy(slot).start()
        c_copy(slot).start()

    def relay(number):
        for other in (side, 1 - side):
            slot = 2 * number + other
            x_copy(slot).wait_recv()
            d_copy(slot).start()

    def expert(number, begin):
        own_rows = pl.ds(pl.multiple_of(number * CAP, CAP), CAP)
        taken = pieces[:, pl.ds(begin, 2), own_rows, :].reshape(n_tp * 2 * CAP, width)
        gate = jnp.dot(taken, gate_w[number], preferred_element_type=jnp.float32)
        upward = jnp.dot(taken, up_w[number], preferred_element_type=jnp.float32)
        hidden = (gate / (1.0 + jnp.exp(-gate)) * upward).astype(jnp.bfloat16)
        columns = min(width, 512)
        for begin_column in range(0, width, columns):
            lanes = slice(begin_column, begin_column + columns)
            result = lax.dot_general(
                hidden,
                down_w[number, lanes, :],
                (((1,), (1,)), ((), ())),
                preferred_element_type=jnp.float32,
            )
            sums[:, pl.ds(begin, 2), own_rows, lanes] = result.astype(jnp.bfloat16).reshape(
                n_tp, 2, CAP, columns
            )

    def experts(number):
        relay(number)
        for slot in (2 * number, 2 * number + 1):
            c_copy(slot).wait_recv()
            d_copy(slot).wait_recv()
        each(0, local, lambda which: expert(which, 2 * number))
        for slot in (2 * number, 2 * number + 1):
            far_copy(slot).start()
            own_copy(slot).start()

    def add(number):
        for other in (1 - side, side):
            slot = 2 * number + other
            far_copy(slot).wait_recv()
            sum_x[slot] = (
                sums[across, slot].astype(jnp.float32) + near_far[slot].astype(jnp.float32)
            ).astype(jnp.bfloat16)
            y_copy(slot).start()

    def total_of(slot):
        own_copy(slot).wait_recv()
        y_copy(slot).wait_recv()
        return (
            sums[tp, slot].astype(jnp.float32)
            + near_own[slot].astype(jnp.float32)
            + got_x[slot].astype(jnp.float32)
        ).astype(jnp.bfloat16)

    def send_back(number, other):
        slot = 2 * number + other
        sum_r[slot] = total_of(slot)
        r_copy(slot, 2 * level_of(number) + other).start()

    tile = rows // 2

    def block(source, keys_ref, diagonal):
        keys = keys_ref[:, :head_dim]
        vals = keys_ref[:, head_dim:]
        at = pl.ds(pl.multiple_of(source * rows, rows), rows)
        for head in range(heads):
            key_gate = forget[head : head + 1, at]
            for piece in range(2):
                span = pl.ds(head * rows + piece * tile, tile)
                scores = lax.dot_general(
                    q[span, :], keys, (((1,), (1,)), ((), ())), preferred_element_type=jnp.float32
                )
                scores = scores * scale + fq[span, 0:1] - key_gate
                if diagonal:
                    qpos = piece * tile + lax.broadcasted_iota(jnp.int32, scores.shape, 0)
                    kpos = lax.broadcasted_iota(jnp.int32, scores.shape, 1)
                    scores = jnp.where(kpos <= qpos, scores, NEGATIVE)
                top = jnp.max(scores, axis=1, keepdims=True)
                if diagonal:
                    newest = top
                else:
                    before = high[span, :]
                    newest = jnp.maximum(before, top)
                weights = jnp.exp(scores - newest)
                total = jnp.sum(weights, axis=1, keepdims=True)
                product = jnp.dot(
                    weights.astype(jnp.bfloat16), vals, preferred_element_type=jnp.float32
                )
                if not diagonal:
                    factor = jnp.exp(before - newest)
                    total = denom[span, :] * factor + total
                    product = accum[span, :] * factor + product
                high[span, :] = newest
                denom[span, :] = total
                accum[span, :] = product

    def keys_on(k):
        lower = ep - 2 * k
        side_copy(kv, lower).wait_recv()
        side_copy(kvbuf.at[lower], lower).start()

        @pl.when(level + 1 < levels)
        def _():
            up_copy(kvbuf.at[lower], lower).start()

    def attend(k):
        lower = ep - 2 * k
        block(lower, kvbuf.at[lower], False)
        other = 2 * (level - k) + 1 - side
        side_copy(kv, other).wait_recv()
        block(other, kvbuf.at[other], False)

    hand_out(level, 0)

    kv[:, :head_dim] = normed_rows(keys_in, slice(None), key_gain[...])
    kv[:, head_dim:] = values_in[...]

    @pl.when(side == 0)
    def _():
        side_copy(kv, ep).start()

    @pl.when(level == 0)
    def _():
        up_copy(kv, ep).start()

    mine = pl.ds(pl.multiple_of(ep * rows, rows), rows)
    for head in range(heads):
        lines = slice(head * rows, (head + 1) * rows)
        lanes = slice(head * head_dim, (head + 1) * head_dim)
        q[lines, :] = normed_rows(queries, lanes, query_gain[...])
        fq[lines, :] = jnp.broadcast_to(forget[head : head + 1, mine], (head_dim, rows)).T

    from_side(0)
    block(ep, kv, True)

    @pl.when(side == 1)
    def _():
        side_copy(kv, ep - 1).wait_recv()
        block(ep - 1, kvbuf.at[ep - 1], False)

    def reach(k):
        low, top = level - k, level + k
        low_at = jnp.where(k <= both, 2 * k - 1, both + k)
        top_at = jnp.where(k <= both, 2 * k, both + k)

        @pl.when(low >= 0)
        def _():
            m_up(low).wait_recv()
            z_up(low).wait_recv()

            @pl.when(level + 1 < levels)
            def _():
                m_up(low).start()
                z_up(low).start()

                @pl.when(low == 0)
                def _():
                    up_copy(kv, ep).start()

        @pl.when(top < levels)
        def _():
            m_down(top).wait_recv()
            z_down(top).wait_recv()

            @pl.when(level > 0)
            def _():
                m_down(top).start()
                z_down(top).start()

        @pl.when(low >= 0)
        def _():
            hand_out(low, low_at)

        @pl.when(top < levels)
        def _():
            hand_out(top, top_at)

        @pl.when(k == 1)
        def _():
            for load in loads:
                load.wait()

        @pl.when(k != 2)
        def _():
            experts(jnp.maximum(k - 2, 0))

        @pl.when(low >= 0)
        def _():
            from_side(low_at)

        @pl.when(top < levels)
        def _():
            from_side(top_at)

    each(1, levels, reach)

    @pl.when(level + 1 < levels)
    def _():
        each(1, level + 1, keys_on)

    def last(number):
        experts(number)
        add(number)

    each(levels - 2, levels, last)
    each(1, levels - 2, add)
    add(0)

    @pl.when(level + 1 == levels)
    def _():
        each(1, level + 1, keys_on)

    def turn(step):
        return jnp.where(step < 2, levels - 2 + step, step - 1)

    def send_both(step):
        number = turn(step)
        send_back(number, 1 - side)
        send_back(number, side)

    def early(step):
        send_both(step)
        for k in (2 * step + 1, 2 * step + 2):

            @pl.when(k <= level)
            def _():
                attend(k)

    each(0, levels // 2, early)
    for head in range(heads):
        span = pl.ds(head * rows, rows)
        result = (accum[span, :] / denom[span, :]).astype(jnp.bfloat16)
        for owner in range(n_tp):
            att[owner, head] = result[owner * part : (owner + 1) * part]
    for step in range(1, n_tp):
        t_copy(tp, step).start()
    att_all[tp] = att[tp]

    each(levels // 2, levels - 1, send_both)

    for step in range(1, n_tp):
        t_copy(lax.rem(tp - step + n_tp, n_tp), step).wait()
    total = None
    for source in range(n_tp):
        for head in range(heads):
            number = source * heads + head
            term = jnp.dot(
                att_all[source, head],
                mixer[number * head_dim : (number + 1) * head_dim, :],
                preferred_element_type=jnp.float32,
            )
            total = term if total is None else total + term
    mixed[...] = total.astype(jnp.bfloat16)

    send_back(0, 1 - side)
    back[ep] = total_of(side)

    def sent(slot):
        x_copy(slot).wait_send()
        c_copy(slot).wait_send()
        d_copy(slot).wait_send()
        far_copy(slot).wait_send()
        own_copy(slot).wait_send()
        y_copy(slot).wait_send()

        @pl.when(slot != side)
        def _():
            r_copy(slot, beside).wait_send()

    each(0, n_ep, sent)
    each(0, levels, lambda number: b_copy(number).wait_send())

    def passed(source):
        @pl.when(jnp.logical_and(source <= level, level + 1 < levels))
        def _():
            m_up(source).wait_send()
            z_up(source).wait_send()

        @pl.when(jnp.logical_and(source >= level, level > 0))
        def _():
            m_down(source).wait_send()
            z_down(source).wait_send()

    each(0, levels, passed)

    @pl.when(level + 1 < levels)
    def _():
        up_copy(kv, ep).wait_send()

    @pl.when(side == 0)
    def _():
        side_copy(kv, ep).wait_send()

    def keys_sent(k):
        source = ep - 2 * k
        side_copy(kv, source).wait_send()

        @pl.when(level + 1 < levels)
        def _():
            up_copy(kv, source).wait_send()

    each(1, level + 1, keys_sent)

    def arrived(source):
        @pl.when(source != ep)
        def _():
            r_arrived(source).wait_recv()

    each(0, n_ep, arrived)

    found_rows = back[...].reshape(n_ep * per, width)
    columns = jnp.concatenate(
        [meta[level, :choices, :], route_weights[...], jnp.zeros((8 - 2 * choices, tokens), jnp.float32)],
        axis=0,
    ).T
    lanes = lax.broadcasted_iota(jnp.int32, (tokens, n_ep * per), 1).astype(jnp.float32)
    summed = None
    for k in range(choices):
        pick = jnp.where(lanes == columns[:, k : k + 1], 1.0, 0.0).astype(jnp.bfloat16)
        found = jnp.dot(pick, found_rows, preferred_element_type=jnp.float32)
        term = found * columns[:, choices + k : choices + k + 1]
        summed = term if summed is None else summed + term
    routed[...] = summed.astype(jnp.bfloat16)


def on_device(
    n_ep,
    n_tp,
    queries,
    keys,
    values,
    forget_cache,
    query_gain,
    key_gain,
    mixer_out,
    expert_input,
    norm_gain,
    routes,
    route_weights,
    w_gate,
    w_up,
    w_down,
):
    rows, head_dim = keys.shape
    heads = forget_cache.shape[0]
    local, width, ff = w_gate.shape
    tokens = expert_input.shape[0]
    per = local * CAP
    part = rows // n_tp
    levels = n_ep // 2
    vmem = pl.BlockSpec(memory_space=pltpu.VMEM)
    anywhere = pl.BlockSpec(memory_space=pl.ANY)
    dma = pltpu.SemaphoreType.DMA
    buffer = pltpu.VMEM((n_ep, per, width), jnp.bfloat16)
    return pl.pallas_call(
        functools.partial(layer_kernel, n_ep, n_tp),
        out_shape=(
            jax.ShapeDtypeStruct((part, width), jnp.bfloat16),
            jax.ShapeDtypeStruct((tokens, width), jnp.bfloat16),
        ),
        in_specs=[vmem] * 10 + [anywhere] * 4,
        out_specs=(vmem, vmem),
        scratch_shapes=[pltpu.VMEM(w_gate.shape, jnp.bfloat16)] * 3
        + [
            pltpu.VMEM(mixer_out.shape, jnp.bfloat16),
            pltpu.VMEM((rows, 2 * head_dim), jnp.bfloat16),
            pltpu.VMEM((n_ep, rows, 2 * head_dim), jnp.bfloat16),
            pltpu.VMEM((heads * rows, head_dim), jnp.bfloat16),
            pltpu.VMEM((heads * rows, head_dim), jnp.float32),
            pltpu.VMEM((levels, tokens, width), jnp.bfloat16),
            pltpu.VMEM((levels, 8, tokens), jnp.float32),
            pltpu.VMEM((levels, per, width), jnp.bfloat16),
            pltpu.VMEM((n_tp, heads, part, head_dim), jnp.bfloat16),
            pltpu.VMEM((n_tp, heads, part, head_dim), jnp.bfloat16),
            pltpu.VMEM((heads * rows, 1), jnp.float32),
            pltpu.VMEM((heads * rows, 1), jnp.float32),
            pltpu.VMEM((heads * rows, head_dim), jnp.float32),
            pltpu.VMEM((n_tp, n_ep, per, width), jnp.bfloat16),
            pltpu.VMEM((n_tp, n_ep, per, width), jnp.bfloat16),
        ]
        + [buffer] * 6
        + [dma((n_ep,))] * 14
        + [dma((levels,))] * 8
        + [dma((n_ep,))] * 3
        + [dma((n_tp,))] * 2
        + [dma((4,))],
        compiler_params=pltpu.CompilerParams(
            collective_id=0, has_side_effects=True, vmem_limit_bytes=VMEM_LIMIT
        ),
        name="layer",
    )(
        expert_input,
        norm_gain.reshape(1, width),
        routes.T,
        route_weights.T,
        queries,
        keys,
        values,
        forget_cache,
        query_gain.reshape(1, head_dim),
        key_gain.reshape(1, head_dim),
        w_gate,
        w_up,
        w_down,
        mixer_out,
    )


def solution(mesh):
    n_ep, n_tp = mesh.shape["ep"], mesh.shape["tp"]
    in_specs = (
        P("ep", "tp"),
        P("ep", "tp"),
        P("ep", "tp"),
        P("tp", None),
        P(),
        P(),
        P(),
        P(("ep", "tp"), None),
        P(),
        P(("ep", "tp"), None),
        P(("ep", "tp"), None),
        P("ep", None, "tp"),
        P("ep", None, "tp"),
        P("ep", None, "tp"),
    )
    out_specs = (P(("ep", "tp"), None), P(("ep", "tp"), None))
    return jax.shard_map(
        functools.partial(on_device, n_ep, n_tp),
        mesh=mesh,
        in_specs=in_specs,
        out_specs=out_specs,
        check_vma=False,
    )
```

time: 164 us -> 127 us (0.77)
  the two profiles are of different devices: /device:TPU:22 before, /device:TPU:0 now
where the time goes in v1:
time: 127 us; the launch traced here: 126 us
  Pallas kernels  122 us (96%)
  local copies, waits for them, and re-layouts  3.76 us (3%)
    pallas_call x1, Pallas kernels, on_device(): pl.pallas_call(functools.partial(layer_kernel, n_ep, n_tp), out_shape=(ja...  122 us
    unnamed x2, local copies, waits for them, and re-layouts  3.76 us

profile of v1, /device:TPU:0, one launch (start us, length us, event | category | flops | bytes accessed | tf_op | source)
XLA Modules:
  0.0 126.4 jit_solution(13592629356125057184)
XLA Ops:
  0.6 122.0 %layer.1 = (bf16[128,2048]{1,0:T(8,128)(2,1)}, bf16[128,2048]{1,0:T(8,128)(2,1)}) custom-call(bf16[128,2048]{1,0:T(8,128)(2,1)} %tokens_in.1, f32[1,2048]{1,0:T(1,128)} %bitcast.5, s32[2,128]{1,0:T(2,128)} %bitcast.6, f32[2,128]{1,0:T(2,128)} %bitcast.7, bf16[512,256]{1,0:T(8,128)(2,1)} %queries.1, bf16[512,128]{1,0:T(8,128)(2,1)} %keys_in.1, ...), custom_call_target="tpu_custom_call" | custom-call | tf_op jit(solution)/shard_map/layer/pallas_call | solution.py:627
  122.7 1.9 %copy.18 = bf16[128,2048]{1,0:T(8,128)(2,1)} copy(bf16[128,2048]{1,0:T(8,128)(2,1)} %get-tuple-element.4) | data formatting | bytes 1048576
  124.5 1.9 %copy.19 = bf16[128,2048]{1,0:T(8,128)(2,1)} copy(bf16[128,2048]{1,0:T(8,128)(2,1)} %get-tuple-element.5) | data formatting | bytes 1048576

commit v2 on v1

--- a/solution.py
+++ b/solution.py
@@ -105,6 +105,10 @@
     t_send,
     t_recv,
     w_sem,
+    mixed_v,
+    routed_v,
+    picked,
+    o_sem,
 ):
     ep, tp, core, across, corner = places(n_tp)
     rows, head_dim = keys_in.shape
@@ -122,6 +126,7 @@
     below = lax.rem(ep + n_ep - 2, n_ep)
     both = jnp.minimum(level, levels - 1 - level)
     assert levels >= 4
+    halves = [slice(0, width // 2), slice(width // 2, width)]
 
     loads = [
         pltpu.make_async_copy(src, dst, w_sem.at[number])
@@ -157,11 +162,15 @@
         lone = jnp.where(level < levels - 1 - level, level + far, level - far)
         return jnp.where(number <= 2 * both, paired, lone)
 
-    def z_up(source):
-        return remote(tok.at[source], tok.at[source], zu_send.at[source], z_recv.at[source], above, tp)
-
-    def z_down(source):
-        return remote(tok.at[source], tok.at[source], zd_send.at[source], z_recv.at[source], below, tp)
+    def z_up(source, half):
+        lines = tok.at[source, :, halves[half]]
+        number = 2 * source + half
+        return remote(lines, lines, zu_send.at[number], z_recv.at[number], above, tp)
+
+    def z_down(source, half):
+        lines = tok.at[source, :, halves[half]]
+        number = 2 * source + half
+        return remote(lines, lines, zd_send.at[number], z_recv.at[number], below, tp)
 
     def m_up(source):
         return remote(meta.at[source], meta.at[source], mu_send.at[source], m_recv.at[source], above, tp)
@@ -169,10 +178,16 @@
     def m_down(source):
         return remote(meta.at[source], meta.at[source], md_send.at[source], m_recv.at[source], below, tp)
 
-    def b_copy(number):
+    def b_copy(number, half):
         slot = 2 * number + side
+        piece = 2 * number + half
         return remote(
-            ysend.at[number], pieces.at[tp, slot], b_send.at[number], b_recv.at[number], beside, tp
+            ysend.at[number, :, halves[half]],
+            pieces.at[tp, slot, :, halves[half]],
+            b_send.at[piece],
+            b_recv.at[piece],
+            beside,
+            tp,
         )
 
     def up_copy(src, source):
@@ -181,15 +196,13 @@
     def side_copy(src, source):
         return remote(src, kvbuf.at[source], k_send.at[source], k_recv.at[source], beside, tp)
 
-    def x_copy(slot):
-        return remote(
-            pieces.at[tp, slot], pieces.at[tp, slot], x_send.at[slot], x_recv.at[slot], ep, across
-        )
-
-    def c_copy(slot):
-        return remote(
-            pieces.at[tp, slot], pieces.at[tp, slot], c_send.at[slot], c_recv.at[slot], ep, core
-        )
+    def x_copy(slot, lanes=slice(None)):
+        piece = pieces.at[tp, slot, :, lanes]
+        return remote(piece, piece, x_send.at[slot], x_recv.at[slot], ep, across)
+
+    def c_copy(slot, lanes=slice(None)):
+        piece = pieces.at[tp, slot, :, lanes]
+        return remote(piece, piece, c_send.at[slot], c_recv.at[slot], ep, core)
 
     def d_copy(slot):
         return remote(
@@ -241,35 +254,39 @@
     @pl.when(level + 1 < levels)
     def _():
         m_up(level).start()
-        z_up(level).start()
+        for half in range(2):
+            z_up(level, half).start()
 
     @pl.when(level > 0)
     def _():
         m_down(level).start()
-        z_down(level).start()
-
-    def select(source, place):
+        for half in range(2):
+            z_down(level, half).start()
+
+    def select(source, place, lanes):
         lines = place * per + lax.broadcasted_iota(jnp.int32, (per, tokens), 0)
         lines = lines.astype(jnp.float32)
         picks = functools.reduce(
             jnp.logical_or, [lines == meta[source, k : k + 1, :] for k in range(choices)]
         )
         picks = jnp.where(picks, 1.0, 0.0).astype(jnp.bfloat16)
-        return jnp.dot(picks, tok[source], preferred_element_type=jnp.float32).astype(jnp.bfloat16)
-
-    def hand_out(source, number):
+        found = jnp.dot(picks, tok[source, :, lanes], preferred_element_type=jnp.float32)
+        return found.astype(jnp.bfloat16)
+
+    def hand_out(source, number, half):
         slot = 2 * number + side
-        pieces[tp, slot] = select(source, ep)
-        x_copy(slot).start()
-        c_copy(slot).start()
-        ysend[number] = select(source, beside)
-        b_copy(number).start()
-
-    def from_side(number):
+        lanes = halves[half]
+        ysend[number, :, lanes] = select(source, beside, lanes)
+        b_copy(number, half).start()
+        pieces[tp, slot, :, lanes] = select(source, ep, lanes)
+        x_copy(slot, lanes).start()
+        c_copy(slot, lanes).start()
+
+    def from_side(number, half):
         slot = 2 * number + 1 - side
-        b_copy(number).wait_recv()
-        x_copy(slot).start()
-        c_copy(slot).start()
+        b_copy(number, half).wait_recv()
+        x_copy(slot, halves[half]).start()
+        c_copy(slot, halves[half]).start()
 
     def relay(number):
         for other in (side, 1 - side):
@@ -297,7 +314,6 @@
             )
 
     def experts(number):
-        relay(number)
         for slot in (2 * number, 2 * number + 1):
             c_copy(slot).wait_recv()
             d_copy(slot).wait_recv()
@@ -378,18 +394,17 @@
     def attend(k):
         lower = ep - 2 * k
         block(lower, kvbuf.at[lower], False)
+
+    def attend_beside(k):
         other = 2 * (level - k) + 1 - side
         side_copy(kv, other).wait_recv()
         block(other, kvbuf.at[other], False)
 
-    hand_out(level, 0)
+    for half in range(2):
+        hand_out(level, 0, half)
 
     kv[:, :head_dim] = normed_rows(keys_in, slice(None), key_gain[...])
     kv[:, head_dim:] = values_in[...]
-
-    @pl.when(side == 0)
-    def _():
-        side_copy(kv, ep).start()
 
     @pl.when(level == 0)
     def _():
@@ -402,103 +417,122 @@
         q[lines, :] = normed_rows(queries, lanes, query_gain[...])
         fq[lines, :] = jnp.broadcast_to(forget[head : head + 1, mine], (head_dim, rows)).T
 
-    from_side(0)
+    for half in range(2):
+        from_side(0, half)
     block(ep, kv, True)
 
-    @pl.when(side == 1)
-    def _():
-        side_copy(kv, ep - 1).wait_recv()
-        block(ep - 1, kvbuf.at[ep - 1], False)
+    def pass_on(k, half):
+        low, top = level - k, level + k
+
+        @pl.when(low >= 0)
+        def _():
+            if half == 0:
+                m_up(low).wait_recv()
+            z_up(low, half).wait_recv()
+
+            @pl.when(level + 1 < levels)
+            def _():
+                if half == 0:
+                    m_up(low).start()
+                z_up(low, half).start()
+
+        @pl.when(top < levels)
+        def _():
+            if half == 0:
+                m_down(top).wait_recv()
+            z_down(top, half).wait_recv()
+
+            @pl.when(level > 0)
+            def _():
+                if half == 0:
+                    m_down(top).start()
+                z_down(top, half).start()
+
+        if half == 1:
+
+            @pl.when(jnp.logical_and(low == 0, level + 1 < levels))
+            def _():
+                up_copy(kv, ep).start()
 
     def reach(k):
         low, top = level - k, level + k
-        low_at = jnp.where(k <= both, 2 * k - 1, both + k)
-        top_at = jnp.where(k <= both, 2 * k, both + k)
-
-        @pl.when(low >= 0)
-        def _():
-            m_up(low).wait_recv()
-            z_up(low).wait_recv()
-
-            @pl.when(level + 1 < levels)
+        first = jnp.where(k <= both, 2 * k - 1, both + k)
+        for half in range(2):
+            pass_on(k, half)
+
+            @pl.when(low >= 0)
             def _():
-                m_up(low).start()
-                z_up(low).start()
-
-                @pl.when(low == 0)
+                hand_out(low, first, half)
+
+            @pl.when(top < levels)
+            def _():
+                hand_out(top, jnp.where(k <= both, 2 * k, both + k), half)
+
+            if half == 0:
+
+                @pl.when(k > 2)
                 def _():
-                    up_copy(kv, ep).start()
-
-        @pl.when(top < levels)
-        def _():
-            m_down(top).wait_recv()
-            z_down(top).wait_recv()
-
-            @pl.when(level > 0)
+                    experts(k - 2)
+
+            if half == 1:
+                relay(k - 1)
+
+                @pl.when(k == 1)
+                def _():
+                    for load in loads:
+                        load.wait()
+
+                @pl.when(jnp.logical_or(k == 1, k == levels - 1))
+                def _():
+                    experts(k - 1)
+
+                interior = jnp.logical_and(k > level, k <= 2 * level)
+
+                @pl.when(jnp.logical_and(level + 1 < levels, interior))
+                def _():
+                    keys_on(k - level)
+
+            @pl.when(jnp.logical_or(low >= 0, top < levels))
             def _():
-                m_down(top).start()
-                z_down(top).start()
-
-        @pl.when(low >= 0)
-        def _():
-            hand_out(low, low_at)
-
-        @pl.when(top < levels)
-        def _():
-            hand_out(top, top_at)
-
-        @pl.when(k == 1)
-        def _():
-            for load in loads:
-                load.wait()
-
-        @pl.when(k != 2)
-        def _():
-            experts(jnp.maximum(k - 2, 0))
-
-        @pl.when(low >= 0)
-        def _():
-            from_side(low_at)
-
-        @pl.when(top < levels)
-        def _():
-            from_side(top_at)
+                from_side(first, half)
+
+            @pl.when(k <= both)
+            def _():
+                from_side(2 * k, half)
 
     each(1, levels, reach)
+
+    @pl.when(side == 0)
+    def _():
+        side_copy(kv, ep).start()
 
     @pl.when(level + 1 < levels)
     def _():
-        each(1, level + 1, keys_on)
-
-    def last(number):
-        experts(number)
-        add(number)
-
-    each(levels - 2, levels, last)
-    each(1, levels - 2, add)
-    add(0)
-
-    @pl.when(level + 1 == levels)
-    def _():
-        each(1, level + 1, keys_on)
-
-    def turn(step):
-        return jnp.where(step < 2, levels - 2 + step, step - 1)
-
-    def send_both(step):
-        number = turn(step)
+        each(jnp.maximum(levels - level, 1), level + 1, keys_on)
+
+    def send_both(number):
         send_back(number, 1 - side)
         send_back(number, side)
 
-    def early(step):
-        send_both(step)
-        for k in (2 * step + 1, 2 * step + 2):
-
-            @pl.when(k <= level)
-            def _():
-                attend(k)
-
-    each(0, levels // 2, early)
+    def top_keys(begin, end):
+        @pl.when(level + 1 == levels)
+        def _():
+            each(begin, end, keys_on)
+
+    add(levels - 2)
+    top_keys(1, levels // 2)
+    relay(levels - 1)
+    experts(levels - 1)
+    send_back(levels - 2, 1 - side)
+    add(levels - 1)
+    each(1, levels - 2, add)
+    send_back(levels - 2, side)
+    top_keys(levels // 2, levels)
+    each(1, level + 1, attend)
+    send_back(levels - 1, 1 - side)
+    each(1 - side, lax.div(level, 2) + 1, attend_beside)
+    send_back(levels - 1, side)
+    each(lax.div(level, 2) + 1, level + 1, attend_beside)
     for head in range(heads):
         span = pl.ds(head * rows, rows)
         result = (accum[span, :] / denom[span, :]).astype(jnp.bfloat16)
@@ -507,25 +541,58 @@
     for step in range(1, n_tp):
         t_copy(tp, step).start()
     att_all[tp] = att[tp]
-
-    each(levels // 2, levels - 1, send_both)
+    add(0)
+    each(1, levels - 2, send_both)
 
     for step in range(1, n_tp):
         t_copy(lax.rem(tp - step + n_tp, n_tp), step).wait()
-    total = None
-    for source in range(n_tp):
-        for head in range(heads):
-            number = source * heads + head
-            term = jnp.dot(
-                att_all[source, head],
-                mixer[number * head_dim : (number + 1) * head_dim, :],
-                preferred_element_type=jnp.float32,
-            )
-            total = term if total is None else total + term
-    mixed[...] = total.astype(jnp.bfloat16)
+    chunk = min(width, 512)
+    strips = [slice(begin, begin + chunk) for begin in range(0, width, chunk)]
+    for lanes in strips:
+        total = None
+        for source in range(n_tp):
+            for head in range(heads):
+                number = source * heads + head
+                term = jnp.dot(
+                    att_all[source, head],
+                    mixer[number * head_dim : (number + 1) * head_dim, lanes],
+                    preferred_element_type=jnp.float32,
+                )
+                total = term if total is None else total + term
+        mixed_v[:, lanes] = total.astype(jnp.bfloat16)
+    mixed_out = pltpu.make_async_copy(mixed_v, mixed, o_sem.at[len(strips)])
+    mixed_out.start()
+
+    columns = jnp.concatenate(
+        [meta[level, :choices, :], route_weights[...], jnp.zeros((8 - 2 * choices, tokens), jnp.float32)],
+        axis=0,
+    ).T
+    slots = lax.broadcasted_iota(jnp.int32, (tokens, n_ep * per), 1).astype(jnp.float32)
+    for k in range(choices):
+        picked[k] = jnp.where(slots == columns[:, k : k + 1], 1.0, 0.0).astype(jnp.bfloat16)
 
     send_back(0, 1 - side)
     back[ep] = total_of(side)
+
+    def arrived(source):
+        @pl.when(source != ep)
+        def _():
+            r_arrived(source).wait_recv()
+
+    each(0, n_ep, arrived)
+
+    outs = []
+    for strip_number, lanes in enumerate(strips):
+        found_rows = back[:, :, lanes].reshape(n_ep * per, chunk)
+        summed = None
+        for k in range(choices):
+            found = jnp.dot(picked[k], found_rows, preferred_element_type=jnp.float32)
+            term = found * columns[:, choices + k : choices + k + 1]
+            summed = term if summed is None else summed + term
+        routed_v[:, lanes] = summed.astype(jnp.bfloat16)
+        out = pltpu.make_async_copy(routed_v.at[:, lanes], routed.at[:, lanes], o_sem.at[strip_number])
+        out.start()
+        outs.append(out)
 
     def sent(slot):
         x_copy(slot).wait_send()
@@ -540,18 +607,21 @@
             r_copy(slot, beside).wait_send()
 
     each(0, n_ep, sent)
-    each(0, levels, lambda number: b_copy(number).wait_send())
+    for half in range(2):
+        each(0, levels, lambda number: b_copy(number, half).wait_send())
 
     def passed(source):
         @pl.when(jnp.logical_and(source <= level, level + 1 < levels))
         def _():
             m_up(source).wait_send()
-            z_up(source).wait_send()
+            for half in range(2):
+                z_up(source, half).wait_send()
 
         @pl.when(jnp.logical_and(source >= level, level > 0))
         def _():
             m_down(source).wait_send()
-            z_down(source).wait_send()
+            for half in range(2):
+                z_down(source, half).wait_send()
 
     each(0, levels, passed)
 
@@ -573,26 +643,34 @@
 
     each(1, level + 1, keys_sent)
 
-    def arrived(source):
-        @pl.when(source != ep)
-        def _():
-            r_arrived(source).wait_recv()
-
-    each(0, n_ep, arrived)
-
-    found_rows = back[...].reshape(n_ep * per, width)
-    columns = jnp.concatenate(
-        [meta[level, :choices, :], route_weights[...], jnp.zeros((8 - 2 * choices, tokens), jnp.float32)],
-        axis=0,
-    ).T
-    lanes = lax.broadcasted_iota(jnp.int32, (tokens, n_ep * per), 1).astype(jnp.float32)
-    summed = None
-    for k in range(choices):
-        pick = jnp.where(lanes == columns[:, k : k + 1], 1.0, 0.0).astype(jnp.bfloat16)
-        found = jnp.dot(pick, found_rows, preferred_element_type=jnp.float32)
-        term = found * columns[:, choices + k : choices + k + 1]
-        summed = term if summed is None else summed + term
-    routed[...] = summed.astype(jnp.bfloat16)
+    mixed_out.wait()
+    for out in outs:
+        out.wait()
+
+
+def hand_off(mixed, routed, mixed_out, routed_out, mixed_v, routed_v, in_sem, out_sem):
+    parts = 2
+    moves = []
+    for which, (src, held, dst) in enumerate(
+        [(mixed, mixed_v, mixed_out), (routed, routed_v, routed_out)]
+    ):
+        lines = src.shape[0] // parts
+        for number in range(parts):
+            span = slice(number * lines, (number + 1) * lines)
+            at = which * parts + number
+            moves.append(
+                (
+                    pltpu.make_async_copy(src.at[span], held.at[span], in_sem.at[at]),
+                    pltpu.make_async_copy(held.at[span], dst.at[span], out_sem.at[at]),
+                )
+            )
+    for load, _ in moves:
+        load.start()
+    for load, store in moves:
+        load.wait()
+        store.start()
+    for _, store in moves:
+        store.wait()
 
 
 def on_device(
@@ -624,14 +702,14 @@
     anywhere = pl.BlockSpec(memory_space=pl.ANY)
     dma = pltpu.SemaphoreType.DMA
     buffer = pltpu.VMEM((n_ep, per, width), jnp.bfloat16)
-    return pl.pallas_call(
+    mixed, routed = pl.pallas_call(
         functools.partial(layer_kernel, n_ep, n_tp),
         out_shape=(
             jax.ShapeDtypeStruct((part, width), jnp.bfloat16),
             jax.ShapeDtypeStruct((tokens, width), jnp.bfloat16),
         ),
         in_specs=[vmem] * 10 + [anywhere] * 4,
-        out_specs=(vmem, vmem),
+        out_specs=(anywhere, anywhere),
         scratch_shapes=[pltpu.VMEM(w_gate.shape, jnp.bfloat16)] * 3
         + [
             pltpu.VMEM(mixer_out.shape, jnp.bfloat16),
@@ -651,11 +729,17 @@
             pltpu.VMEM((n_tp, n_ep, per, width), jnp.bfloat16),
         ]
         + [buffer] * 6
-        + [dma((n_ep,))] * 14
-        + [dma((levels,))] * 8
-        + [dma((n_ep,))] * 3
+        + [dma((n_ep,))] * 17
+        + [dma((levels,))] * 3
+        + [dma((n_ep,))] * 5
         + [dma((n_tp,))] * 2
-        + [dma((4,))],
+        + [
+            dma((4,)),
+            pltpu.VMEM((part, width), jnp.bfloat16),
+            pltpu.VMEM((tokens, width), jnp.bfloat16),
+            pltpu.VMEM((routes.shape[1], tokens, n_ep * per), jnp.bfloat16),
+            dma((width // min(width, 512) + 1,)),
+        ],
         compiler_params=pltpu.CompilerParams(
             collective_id=0, has_side_effects=True, vmem_limit_bytes=VMEM_LIMIT
         ),
@@ -676,6 +760,15 @@
         w_down,
         mixer_out,
     )
+    return pl.pallas_call(
+        hand_off,
+        out_shape=tuple(jax.ShapeDtypeStruct(part.shape, part.dtype) for part in (mixed, routed)),
+        in_specs=[anywhere] * 2,
+        out_specs=(anywhere, anywhere),
+        scratch_shapes=[pltpu.VMEM(part.shape, part.dtype) for part in (mixed, routed)]
+        + [dma((4,))] * 2,
+        name="hand_off",
+    )(mixed, routed)
 
 
 def solution(mesh):

time: 127 us -> 113 us (0.89)
  Pallas kernels: 122 us -> 112 us
  local copies, waits for them, and re-layouts: 3.76 us -> 0 us
    pallas_call x1, Pallas kernels: 122 us -> 110 us  [on_device(): pl.pallas_call(functools.partial(layer_kernel, n_ep, n_tp), out_shape=(ja...]
    unnamed x2 -> x0, local copies, waits for them, and re-layouts: 3.76 us -> none
    pallas_call x0 -> x1, Pallas kernels: none -> 1.98 us  [on_device(): pl.pallas_call(hand_off, out_shape=tuple((jax.ShapeDtypeStruct(part.shape...]
where the time goes in v2:
time: 113 us
  Pallas kernels  112 us (99%)
    pallas_call x1, Pallas kernels, on_device(): pl.pallas_call(functools.partial(layer_kernel, n_ep, n_tp), out_shape=(ja...  110 us

profile of v2, /device:TPU:0, one launch (start us, length us, event | category | flops | bytes accessed | tf_op | source)
XLA Modules:
  0.0 112.8 jit_solution(12774710662148625490)
XLA Ops:
  0.6 110.1 %layer.1 = (bf16[128,2048]{1,0:T(8,128)(2,1)}, bf16[128,2048]{1,0:T(8,128)(2,1)}) custom-call(bf16[128,2048]{1,0:T(8,128)(2,1)} %tokens_in.1, f32[1,2048]{1,0:T(1,128)} %bitcast.5, s32[2,128]{1,0:T(2,128)} %bitcast.6, f32[2,128]{1,0:T(2,128)} %bitcast.7, bf16[512,256]{1,0:T(8,128)(2,1)} %queries.1, bf16[512,128]{1,0:T(8,128)(2,1)} %keys_in.1, ...), custom_call_target="tpu_custom_call" | custom-call | tf_op jit(solution)/shard_map/layer/pallas_call | solution.py:705
  110.7 2.0 %hand_off.1 = (bf16[128,2048]{1,0:T(8,128)(2,1)}, bf16[128,2048]{1,0:T(8,128)(2,1)}) custom-call(bf16[128,2048]{1,0:T(8,128)(2,1)} %get-tuple-element.4.mixed, bf16[128,2048]{1,0:T(8,128)(2,1)} %get-tuple-element.5.routed), custom_call_target="tpu_custom_call" | custom-call | tf_op jit(solution)/shard_map/hand_off/pallas_call | solution.py:763

commit v3 on v2

--- a/solution.py
+++ b/solution.py
@@ -11,7 +11,7 @@
 EPSILON = 1e-06
 NEGATIVE = -1e30
 MESH = pl.DeviceIdType.MESH
-VMEM_LIMIT = 62 * 1024 * 1024
+VMEM_LIMIT = 63 * 1024 * 1024
 
 
 def places(n_tp):
@@ -108,7 +108,18 @@
     mixed_v,
     routed_v,
     picked,
+    weighing,
+    gathered,
     o_sem,
+    pair_rows,
+    part_v,
+    far_in,
+    merged,
+    p_send,
+    p_recv,
+    g_send,
+    g_recv,
+    h_recv,
 ):
     ep, tp, core, across, corner = places(n_tp)
     rows, head_dim = keys_in.shape
@@ -125,6 +136,7 @@
     above = lax.rem(ep + 2, n_ep)
     below = lax.rem(ep + n_ep - 2, n_ep)
     both = jnp.minimum(level, levels - 1 - level)
+    edge, joins = both == 0, both <= 1
     assert levels >= 4
     halves = [slice(0, width // 2), slice(width // 2, width)]
 
@@ -164,13 +176,15 @@
 
     def z_up(source, half):
         lines = tok.at[source, :, halves[half]]
-        number = 2 * source + half
-        return remote(lines, lines, zu_send.at[number], z_recv.at[number], above, tp)
+        return remote(lines, lines, zu_send.at[source], z_recv.at[2 * source + half], above, tp)
 
     def z_down(source, half):
         lines = tok.at[source, :, halves[half]]
-        number = 2 * source + half
-        return remote(lines, lines, zd_send.at[number], z_recv.at[number], below, tp)
+        return remote(lines, lines, zd_send.at[source], z_recv.at[2 * source + half], below, tp)
+
+    def passed_all(source, sems):
+        block = tok.at[source]
+        return remote(block, block, sems.at[source], z_recv.at[0], above, tp)
 
     def m_up(source):
         return remote(meta.at[source], meta.at[source], mu_send.at[source], m_recv.at[source], above, tp)
@@ -184,45 +198,71 @@
         return remote(
             ysend.at[number, :, halves[half]],
             pieces.at[tp, slot, :, halves[half]],
-            b_send.at[piece],
+            b_send.at[0],
             b_recv.at[piece],
             beside,
             tp,
         )
 
     def up_copy(src, source):
-        return remote(src, kvbuf.at[source], u_send.at[source], k_recv.at[source], above, tp)
+        return remote(src, kvbuf.at[source], u_send.at[lax.div(source, 2)], k_recv.at[source], above, tp)
 
     def side_copy(src, source):
-        return remote(src, kvbuf.at[source], k_send.at[source], k_recv.at[source], beside, tp)
-
-    def x_copy(slot, lanes=slice(None)):
+        return remote(src, kvbuf.at[source], k_send.at[lax.div(source, 2)], k_recv.at[source], beside, tp)
+
+    def x_move(src, dst, slot):
+        return remote(src, dst, x_send.at[0], x_recv.at[lax.div(slot, 2)], ep, across)
+
+    def c_move(src, dst, slot):
+        return remote(src, dst, c_send.at[0], c_recv.at[lax.div(slot, 2)], ep, core)
+
+    def d_move(src, dst, slot):
+        return remote(src, dst, d_send.at[0], d_recv.at[lax.div(slot, 2)], ep, core)
+
+    def f_move(src, dst, slot):
+        return remote(src, dst, f_send.at[0], f_recv.at[lax.div(slot, 2)], ep, core)
+
+    def n_move(src, dst, slot):
+        return remote(src, dst, n_send.at[0], n_recv.at[lax.div(slot, 2)], ep, core)
+
+    def x_copy(slot, lanes):
         piece = pieces.at[tp, slot, :, lanes]
-        return remote(piece, piece, x_send.at[slot], x_recv.at[slot], ep, across)
-
-    def c_copy(slot, lanes=slice(None)):
+        return x_move(piece, piece, slot)
+
+    def c_copy(slot, lanes):
         piece = pieces.at[tp, slot, :, lanes]
-        return remote(piece, piece, c_send.at[slot], c_recv.at[slot], ep, core)
+        return c_move(piece, piece, slot)
 
     def d_copy(slot):
+        piece = pieces.at[across, slot]
+        return d_move(piece, piece, slot)
+
+    def far_copy(slot):
+        return f_move(sums.at[corner, slot], near_far.at[slot], slot)
+
+    def own_copy(slot):
+        return n_move(sums.at[core, slot], near_own.at[slot], slot)
+
+    def pair(buffer, number):
+        return buffer.at[pl.ds(2 * number, 2)]
+
+    def y_copy(slot, half):
+        lanes, piece = halves[half], 2 * slot + half
         return remote(
-            pieces.at[across, slot], pieces.at[across, slot], d_send.at[slot], d_recv.at[slot], ep, core
+            sum_x.at[slot, :, lanes],
+            got_x.at[slot, :, lanes],
+            y_send.at[0],
+            y_recv.at[piece],
+            ep,
+            across,
         )
 
-    def far_copy(slot):
-        return remote(sums.at[corner, slot], near_far.at[slot], f_send.at[slot], f_recv.at[slot], ep, core)
-
-    def own_copy(slot):
-        return remote(sums.at[core, slot], near_own.at[slot], n_send.at[slot], n_recv.at[slot], ep, core)
-
-    def y_copy(slot):
-        return remote(sum_x.at[slot], got_x.at[slot], y_send.at[slot], y_recv.at[slot], ep, across)
-
-    def r_copy(slot, dest):
-        return remote(sum_r.at[slot], back.at[ep], r_send.at[slot], r_recv.at[ep], dest, tp)
-
-    def r_arrived(source):
-        return remote(sum_r.at[0], back.at[source], r_send.at[0], r_recv.at[source], beside, tp)
+    def r_copy(slot, dest, lanes=slice(None)):
+        src, dst = sum_r.at[slot, :, lanes], back.at[ep, :, lanes]
+        return remote(src, dst, r_send.at[0], r_recv.at[level], dest, tp)
+
+    def r_arrived(rows_of, source):
+        return remote(rows_of, rows_of, r_send.at[0], r_recv.at[source], beside, tp)
 
     def t_copy(source, step):
         dest = lax.rem(tp + step, n_tp)
@@ -248,6 +288,7 @@
     for k in range(choices):
         rank = jnp.sum(jnp.where(named[k], prior, 0.0), axis=0, keepdims=True)
         meta[level, k : k + 1, :] = routes[k : k + 1, :].astype(jnp.float32) * CAP + rank
+    meta[level, choices : 2 * choices, :] = route_weights[...]
 
     pl.semaphore_wait(barrier, n_ep + n_tp - 2)
 
@@ -289,9 +330,9 @@
         c_copy(slot, halves[half]).start()
 
     def relay(number):
-        for other in (side, 1 - side):
-            slot = 2 * number + other
-            x_copy(slot).wait_recv()
+        whole = pair(pieces.at[across], number)
+        x_move(whole, whole, 2 * number).wait_recv()
+        for slot in (2 * number, 2 * number + 1):
             d_copy(slot).start()
 
     def expert(number, begin):
@@ -314,36 +355,119 @@
             )
 
     def experts(number):
-        for slot in (2 * number, 2 * number + 1):
-            c_copy(slot).wait_recv()
-            d_copy(slot).wait_recv()
+        whole = pair(pieces.at[core], number)
+        c_move(whole, whole, 2 * number).wait_recv()
+        d_move(whole, whole, 2 * number).wait_recv()
         each(0, local, lambda which: expert(which, 2 * number))
         for slot in (2 * number, 2 * number + 1):
             far_copy(slot).start()
             own_copy(slot).start()
 
     def add(number):
+        whole = pair(near_far, number)
+        f_move(whole, whole, 2 * number).wait_recv()
         for other in (1 - side, side):
             slot = 2 * number + other
-            far_copy(slot).wait_recv()
-            sum_x[slot] = (
-                sums[across, slot].astype(jnp.float32) + near_far[slot].astype(jnp.float32)
-            ).astype(jnp.bfloat16)
-            y_copy(slot).start()
-
-    def total_of(slot):
-        own_copy(slot).wait_recv()
-        y_copy(slot).wait_recv()
+            for half in range(2):
+                lanes = halves[half]
+                sum_x[slot, :, lanes] = (
+                    sums[across, slot, :, lanes].astype(jnp.float32)
+                    + near_far[slot, :, lanes].astype(jnp.float32)
+                ).astype(jnp.bfloat16)
+                y_copy(slot, half).start()
+
+    def own_landed(number, other):
+        @pl.when(other != side)
+        def _():
+            whole = pair(near_own, number)
+            n_move(whole, whole, 2 * number).wait_recv()
+
+    def total_of(slot, half):
+        lanes = halves[half]
+        y_copy(slot, half).wait_recv()
         return (
-            sums[tp, slot].astype(jnp.float32)
-            + near_own[slot].astype(jnp.float32)
-            + got_x[slot].astype(jnp.float32)
+            sums[tp, slot, :, lanes].astype(jnp.float32)
+            + near_own[slot, :, lanes].astype(jnp.float32)
+            + got_x[slot, :, lanes].astype(jnp.float32)
         ).astype(jnp.bfloat16)
 
     def send_back(number, other):
         slot = 2 * number + other
-        sum_r[slot] = total_of(slot)
-        r_copy(slot, 2 * level_of(number) + other).start()
+        own_landed(number, other)
+        for half in range(2):
+            sum_r[slot, :, halves[half]] = total_of(slot, half)
+            r_copy(slot, 2 * level_of(number) + other, halves[half]).start()
+
+    goal = level_of(levels - 1)
+    toward = jnp.where(level == 0, above, below)
+
+    def p_copy(half):
+        src = sum_r.at[2 * levels - 1 - side, :, halves[half]]
+        dst = pair_rows.at[side, :, halves[half]]
+        return remote(src, dst, p_send.at[0], p_recv.at[half], beside, tp)
+
+    def g_copy(half):
+        src, dst = part_v.at[:, halves[half]], far_in.at[:, halves[half]]
+        return remote(src, dst, g_send.at[0], g_recv.at[half], toward, tp)
+
+    def h_copy(half):
+        src, dst = part_v.at[:, halves[half]], merged.at[:, halves[half]]
+        return remote(src, dst, g_send.at[0], h_recv.at[0], 2 * goal + side, tp)
+
+    def weighed(half):
+        p_copy(half).wait_recv()
+        columns = meta[goal].T
+        names = 2 * per * level + lax.broadcasted_iota(jnp.int32, (tokens, 2 * per), 1)
+        names = names.astype(jnp.float32)
+        rows_of = pair_rows[:, :, halves[half]].reshape(2 * per, width // 2)
+        summed = None
+        for k in range(choices):
+            pick = jnp.where(names == columns[:, k : k + 1], 1.0, 0.0).astype(jnp.bfloat16)
+            found = jnp.dot(pick, rows_of, preferred_element_type=jnp.float32)
+            term = found * columns[:, choices + k : choices + k + 1]
+            summed = term if summed is None else summed + term
+        return summed
+
+    def merge_out(half):
+        part_v[:, halves[half]] = weighed(half).astype(jnp.bfloat16)
+        g_copy(half).start()
+
+    def merge_on(half):
+        @pl.when(jnp.logical_and(joins, jnp.logical_not(edge)))
+        def _():
+            summed = weighed(half)
+            g_copy(half).wait_recv()
+            summed = summed + far_in[:, halves[half]].astype(jnp.float32)
+            part_v[:, halves[half]] = summed.astype(jnp.bfloat16)
+            h_copy(half).start()
+
+    def far_first():
+        @pl.when(joins)
+        def _():
+            slot = 2 * levels - 1 - side
+            own_landed(levels - 1, 1 - side)
+            for half in range(2):
+                sum_r[slot, :, halves[half]] = total_of(slot, half)
+                p_copy(half).start()
+
+        @pl.when(jnp.logical_not(joins))
+        def _():
+            send_back(levels - 1, 1 - side)
+
+    def far_second():
+        @pl.when(joins)
+        def _():
+            for half in range(2):
+                pair_rows[side, :, halves[half]] = total_of(2 * levels - 2 + side, half)
+
+        @pl.when(jnp.logical_not(joins))
+        def _():
+            send_back(levels - 1, side)
+
+        @pl.when(edge)
+        def _():
+            for half in range(2):
+                merge_out(half)
 
     tile = rows // 2
 
@@ -469,12 +593,22 @@
                 hand_out(top, jnp.where(k <= both, 2 * k, both + k), half)
 
             if half == 0:
+                interior = jnp.logical_and(k > level, k <= 2 * level)
+
+                @pl.when(jnp.logical_and(level + 1 < levels, interior))
+                def _():
+                    keys_on(k - level)
 
                 @pl.when(k > 2)
                 def _():
                     experts(k - 2)
 
             if half == 1:
+
+                @pl.when(jnp.logical_and(level + 1 < levels, k == levels - 1))
+                def _():
+                    each(jnp.maximum(levels - level, 1), level + 1, keys_on)
+
                 relay(k - 1)
 
                 @pl.when(k == 1)
@@ -486,12 +620,6 @@
                 def _():
                     experts(k - 1)
 
-                interior = jnp.logical_and(k > level, k <= 2 * level)
-
-                @pl.when(jnp.logical_and(level + 1 < levels, interior))
-                def _():
-                    keys_on(k - level)
-
             @pl.when(jnp.logical_or(low >= 0, top < levels))
             def _():
                 from_side(first, half)
@@ -506,10 +634,6 @@
     def _():
         side_copy(kv, ep).start()
 
-    @pl.when(level + 1 < levels)
-    def _():
-        each(jnp.maximum(levels - level, 1), level + 1, keys_on)
-
     def send_both(number):
         send_back(number, 1 - side)
         send_back(number, side)
@@ -519,19 +643,23 @@
         def _():
             each(begin, end, keys_on)
 
-    add(levels - 2)
+    early = jnp.where(both == 1, 1, levels - 2)
+    late = jnp.where(both == 1, levels - 2, 1)
+    add(early)
     top_keys(1, levels // 2)
     relay(levels - 1)
+    top_keys(levels // 2, 3 * levels // 4)
     experts(levels - 1)
-    send_back(levels - 2, 1 - side)
+    send_back(early, 1 - side)
     add(levels - 1)
-    each(1, levels - 2, add)
-    send_back(levels - 2, side)
-    top_keys(levels // 2, levels)
+    add(late)
+    each(2, levels - 2, add)
+    top_keys(3 * levels // 4, levels)
+    send_back(early, side)
     each(1, level + 1, attend)
-    send_back(levels - 1, 1 - side)
+    far_first()
     each(1 - side, lax.div(level, 2) + 1, attend_beside)
-    send_back(levels - 1, side)
+    far_second()
     each(lax.div(level, 2) + 1, level + 1, attend_beside)
     for head in range(heads):
         span = pl.ds(head * rows, rows)
@@ -542,7 +670,11 @@
         t_copy(tp, step).start()
     att_all[tp] = att[tp]
     add(0)
-    each(1, levels - 2, send_both)
+    send_back(late, 1 - side)
+    merge_on(0)
+    send_back(late, side)
+    merge_on(1)
+    each(2, levels - 2, send_both)
 
     for step in range(1, n_tp):
         t_copy(lax.rem(tp - step + n_tp, n_tp), step).wait()
@@ -563,65 +695,90 @@
     mixed_out = pltpu.make_async_copy(mixed_v, mixed, o_sem.at[len(strips)])
     mixed_out.start()
 
-    columns = jnp.concatenate(
-        [meta[level, :choices, :], route_weights[...], jnp.zeros((8 - 2 * choices, tokens), jnp.float32)],
-        axis=0,
-    ).T
-    slots = lax.broadcasted_iota(jnp.int32, (tokens, n_ep * per), 1).astype(jnp.float32)
-    for k in range(choices):
-        picked[k] = jnp.where(slots == columns[:, k : k + 1], 1.0, 0.0).astype(jnp.bfloat16)
+    columns = meta[level].T
+    slots = lax.broadcasted_iota(jnp.int32, (tokens, 2 * per), 1)
+    for lower in range(levels):
+        names = (lower * 2 * per + slots).astype(jnp.float32)
+        for k in range(choices):
+            picked[lower, k] = jnp.where(names == columns[:, k : k + 1], 1.0, 0.0).astype(
+                jnp.bfloat16
+            )
+    weighing[...] = columns
+    gathered[...] = jnp.zeros(gathered.shape, jnp.float32)
+
+    def gather(source, lanes):
+        found_rows = back[pl.ds(2 * source, 2), :, lanes].reshape(2 * per, chunk)
+        summed = gathered[:, lanes]
+        for k in range(choices):
+            found = jnp.dot(picked[source, k], found_rows, preferred_element_type=jnp.float32)
+            summed = summed + found * weighing[:, choices + k : choices + k + 1]
+        return summed
+
+    def far_rows(number):
+        source = level_of(number)
+
+        @pl.when(jnp.logical_not(jnp.logical_and(edge, number >= levels - 2)))
+        def _():
+            r_arrived(pair(back, source), source).wait_recv()
+            for lanes in strips:
+                gathered[:, lanes] = gather(source, lanes)
 
     send_back(0, 1 - side)
-    back[ep] = total_of(side)
-
-    def arrived(source):
-        @pl.when(source != ep)
-        def _():
-            r_arrived(source).wait_recv()
-
-    each(0, n_ep, arrived)
-
+    each(1, levels, far_rows)
+
+    @pl.when(edge)
+    def _():
+        remote(part_v, merged, g_send.at[0], h_recv.at[0], beside, tp).wait_recv()
+        for lanes in strips:
+            gathered[:, lanes] = gathered[:, lanes] + merged[:, lanes].astype(jnp.float32)
+
+    for half in range(2):
+        back[ep, :, halves[half]] = total_of(side, half)
+    r_arrived(back.at[beside], level).wait_recv()
     outs = []
     for strip_number, lanes in enumerate(strips):
-        found_rows = back[:, :, lanes].reshape(n_ep * per, chunk)
-        summed = None
-        for k in range(choices):
-            found = jnp.dot(picked[k], found_rows, preferred_element_type=jnp.float32)
-            term = found * columns[:, choices + k : choices + k + 1]
-            summed = term if summed is None else summed + term
-        routed_v[:, lanes] = summed.astype(jnp.bfloat16)
+        routed_v[:, lanes] = gather(level, lanes).astype(jnp.bfloat16)
         out = pltpu.make_async_copy(routed_v.at[:, lanes], routed.at[:, lanes], o_sem.at[strip_number])
         out.start()
         outs.append(out)
 
-    def sent(slot):
-        x_copy(slot).wait_send()
-        c_copy(slot).wait_send()
-        d_copy(slot).wait_send()
-        far_copy(slot).wait_send()
-        own_copy(slot).wait_send()
-        y_copy(slot).wait_send()
-
-        @pl.when(slot != side)
-        def _():
-            r_copy(slot, beside).wait_send()
-
-    each(0, n_ep, sent)
-    for half in range(2):
-        each(0, levels, lambda number: b_copy(number, half).wait_send())
+    for move, whole in (
+        (x_move, pieces.at[tp]),
+        (c_move, pieces.at[tp]),
+        (d_move, pieces.at[across]),
+        (f_move, sums.at[corner]),
+        (n_move, sums.at[core]),
+    ):
+        move(whole, whole, 0).wait_send()
+    remote(sum_x, got_x, y_send.at[0], y_recv.at[0], ep, across).wait_send()
+
+    def back_sent(count):
+        most = pl.ds(0, count)
+        remote(sum_r.at[most], back.at[most], r_send.at[0], r_recv.at[0], beside, tp).wait_send()
+
+    @pl.when(joins)
+    def _():
+        back_sent(n_ep - 3)
+        src, dst = sum_r.at[0], pair_rows.at[0]
+        remote(src, dst, p_send.at[0], p_recv.at[0], beside, tp).wait_send()
+        remote(part_v, merged, g_send.at[0], h_recv.at[0], beside, tp).wait_send()
+
+    @pl.when(jnp.logical_not(joins))
+    def _():
+        back_sent(n_ep - 1)
+
+    remote(ysend, ysend, b_send.at[0], b_recv.at[0], beside, tp).wait_send()
 
     def passed(source):
         @pl.when(jnp.logical_and(source <= level, level + 1 < levels))
         def _():
             m_up(source).wait_send()
-            for half in range(2):
-                z_up(source, half).wait_send()
+            passed_all(source, zu_send).wait_send()
 
         @pl.when(jnp.logical_and(source >= level, level > 0))
         def _():
             m_down(source).wait_send()
-            for half in range(2):
-                z_down(source, half).wait_send()
+            passed_all(source, zd_send).wait_send()
 
     each(0, levels, passed)
 
@@ -643,9 +800,12 @@
 
     each(1, level + 1, keys_sent)
 
-    mixed_out.wait()
-    for out in outs:
-        out.wait()
+    def finish():
+        mixed_out.wait()
+        for out in outs:
+            out.wait()
+
+    finish()
 
 
 def hand_off(mixed, routed, mixed_out, routed_out, mixed_v, routed_v, in_sem, out_sem):
@@ -729,16 +889,30 @@
             pltpu.VMEM((n_tp, n_ep, per, width), jnp.bfloat16),
         ]
         + [buffer] * 6
-        + [dma((n_ep,))] * 17
+        + [dma((1,)), dma((levels,))] * 5
+        + [dma((1,)), dma((2 * n_ep,)), dma((1,)), dma((levels,))]
+        + [dma((levels,)), dma((levels,)), dma((n_ep,))]
         + [dma((levels,))] * 3
-        + [dma((n_ep,))] * 5
+        + [dma((1,)), dma((n_ep,))]
+        + [dma((levels,)), dma((levels,)), dma((n_ep,))]
         + [dma((n_tp,))] * 2
         + [
             dma((4,)),
             pltpu.VMEM((part, width), jnp.bfloat16),
             pltpu.VMEM((tokens, width), jnp.bfloat16),
-            pltpu.VMEM((routes.shape[1], tokens, n_ep * per), jnp.bfloat16),
+            pltpu.VMEM((levels, routes.shape[1], tokens, 2 * per), jnp.bfloat16),
+            pltpu.VMEM((tokens, 8), jnp.float32),
+            pltpu.VMEM((tokens, width), jnp.float32),
             dma((width // min(width, 512) + 1,)),
+            pltpu.VMEM((2, per, width), jnp.bfloat16),
+        ]
+        + [pltpu.VMEM((tokens, width), jnp.bfloat16)] * 3
+        + [
+            dma((1,)),
+            dma((2,)),
+            dma((1,)),
+            dma((2,)),
+            dma((1,)),
         ],
         compiler_params=pltpu.CompilerParams(
             collective_id=0, has_side_effects=True, vmem_limit_bytes=VMEM_LIMIT

time: 113 us -> 107 us (0.947)
  Pallas kernels: 112 us -> 106 us
    pallas_call x1, Pallas kernels: 110 us -> 105 us  [on_device(): pl.pallas_call(functools.partial(layer_kernel, n_ep, n_tp), out_shape=(ja...]
where the time goes in v3:
time: 107 us
  Pallas kernels  106 us (99%)
    pallas_call x1, Pallas kernels, on_device(): pl.pallas_call(functools.partial(layer_kernel, n_ep, n_tp), out_shape=(ja...  105 us

profile of v3, /device:TPU:0, one launch (start us, length us, event | category | flops | bytes accessed | tf_op | source)
XLA Modules:
  0.0 107.3 jit_solution(9139297409200182166)
XLA Ops:
  0.6 104.5 %layer.1 = (bf16[128,2048]{1,0:T(8,128)(2,1)}, bf16[128,2048]{1,0:T(8,128)(2,1)}) custom-call(bf16[128,2048]{1,0:T(8,128)(2,1)} %tokens_in.1, f32[1,2048]{1,0:T(1,128)} %bitcast.5, s32[2,128]{1,0:T(2,128)} %bitcast.6, f32[2,128]{1,0:T(2,128)} %bitcast.7, bf16[512,256]{1,0:T(8,128)(2,1)} %queries.1, bf16[512,128]{1,0:T(8,128)(2,1)} %keys_in.1, ...), custom_call_target="tpu_custom_call" | custom-call | tf_op jit(solution)/shard_map/layer/pallas_call | solution.py:865
  105.2 2.0 %hand_off.1 = (bf16[128,2048]{1,0:T(8,128)(2,1)}, bf16[128,2048]{1,0:T(8,128)(2,1)}) custom-call(bf16[128,2048]{1,0:T(8,128)(2,1)} %get-tuple-element.4.mixed, bf16[128,2048]{1,0:T(8,128)(2,1)} %get-tuple-element.5.routed), custom_call_target="tpu_custom_call" | custom-call | tf_op jit(solution)/shard_map/hand_off/pallas_call | solution.py:937

commit v4 on v3

--- a/solution.py
+++ b/solution.py
@@ -290,20 +290,6 @@
         meta[level, k : k + 1, :] = routes[k : k + 1, :].astype(jnp.float32) * CAP + rank
     meta[level, choices : 2 * choices, :] = route_weights[...]
 
-    pl.semaphore_wait(barrier, n_ep + n_tp - 2)
-
-    @pl.when(level + 1 < levels)
-    def _():
-        m_up(level).start()
-        for half in range(2):
-            z_up(level, half).start()
-
-    @pl.when(level > 0)
-    def _():
-        m_down(level).start()
-        for half in range(2):
-            z_down(level, half).start()
-
     def select(source, place, lanes):
         lines = place * per + lax.broadcasted_iota(jnp.int32, (per, tokens), 0)
         lines = lines.astype(jnp.float32)
@@ -314,14 +300,39 @@
         found = jnp.dot(picks, tok[source, :, lanes], preferred_element_type=jnp.float32)
         return found.astype(jnp.bfloat16)
 
+    def pick_rows(source, number, half):
+        lanes = halves[half]
+        pieces[tp, 2 * number + side, :, lanes] = select(source, ep, lanes)
+        ysend[number, :, lanes] = select(source, beside, lanes)
+
+    def send_rows(number, half):
+        slot = 2 * number + side
+        x_copy(slot, halves[half]).start()
+        b_copy(number, half).start()
+        c_copy(slot, halves[half]).start()
+
+    for half in range(2):
+        pick_rows(level, 0, half)
+
+    pl.semaphore_wait(barrier, n_ep + n_tp - 2)
+    for half in range(2):
+        send_rows(0, half)
+
+    @pl.when(level + 1 < levels)
+    def _():
+        m_up(level).start()
+        for half in range(2):
+            z_up(level, half).start()
+
+    @pl.when(level > 0)
+    def _():
+        m_down(level).start()
+        for half in range(2):
+            z_down(level, half).start()
+
     def hand_out(source, number, half):
-        slot = 2 * number + side
-        lanes = halves[half]
-        ysend[number, :, lanes] = select(source, beside, lanes)
-        b_copy(number, half).start()
-        pieces[tp, slot, :, lanes] = select(source, ep, lanes)
-        x_copy(slot, lanes).start()
-        c_copy(slot, lanes).start()
+        pick_rows(source, number, half)
+        send_rows(number, half)
 
     def from_side(number, half):
         slot = 2 * number + 1 - side
@@ -524,8 +535,6 @@
         side_copy(kv, other).wait_recv()
         block(other, kvbuf.at[other], False)
 
-    for half in range(2):
-        hand_out(level, 0, half)
 
     kv[:, :head_dim] = normed_rows(keys_in, slice(None), key_gain[...])
     kv[:, head_dim:] = values_in[...]
@@ -732,15 +741,19 @@
         for lanes in strips:
             gathered[:, lanes] = gathered[:, lanes] + merged[:, lanes].astype(jnp.float32)
 
+    r_arrived(back.at[beside], level).wait_recv()
+    outs = []
     for half in range(2):
         back[ep, :, halves[half]] = total_of(side, half)
-    r_arrived(back.at[beside], level).wait_recv()
-    outs = []
-    for strip_number, lanes in enumerate(strips):
-        routed_v[:, lanes] = gather(level, lanes).astype(jnp.bfloat16)
-        out = pltpu.make_async_copy(routed_v.at[:, lanes], routed.at[:, lanes], o_sem.at[strip_number])
-        out.start()
-        outs.append(out)
+        for strip_number, lanes in enumerate(strips):
+            if lanes.start // (width // 2) != half:
+                continue
+            routed_v[:, lanes] = gather(level, lanes).astype(jnp.bfloat16)
+            out = pltpu.make_async_copy(
+                routed_v.at[:, lanes], routed.at[:, lanes], o_sem.at[strip_number]
+            )
+            out.start()
+            outs.append(out)
 
     for move, whole in (
         (x_move, pieces.at[tp]),

time: 107 us -> 107 us (level)
  no operation moved by 1% of the time
where the time goes in v4:
time: 107 us
  Pallas kernels  106 us (99%)
    pallas_call x1, Pallas kernels, on_device(): pl.pallas_call(functools.partial(layer_kernel, n_ep, n_tp), out_shape=(ja...  104 us

profile of v4, /device:TPU:0, one launch (start us, length us, event | category | flops | bytes accessed | tf_op | source)
XLA Modules:
  0.0 106.8 jit_solution(16272265589520801841)
XLA Ops:
  0.6 104.0 %layer.1 = (bf16[128,2048]{1,0:T(8,128)(2,1)}, bf16[128,2048]{1,0:T(8,128)(2,1)}) custom-call(bf16[128,2048]{1,0:T(8,128)(2,1)} %tokens_in.1, f32[1,2048]{1,0:T(1,128)} %bitcast.5, s32[2,128]{1,0:T(2,128)} %bitcast.6, f32[2,128]{1,0:T(2,128)} %bitcast.7, bf16[512,256]{1,0:T(8,128)(2,1)} %queries.1, bf16[512,128]{1,0:T(8,128)(2,1)} %keys_in.1, ...), custom_call_target="tpu_custom_call" | custom-call | tf_op jit(solution)/shard_map/layer/pallas_call | solution.py:878
  104.7 2.0 %hand_off.1 = (bf16[128,2048]{1,0:T(8,128)(2,1)}, bf16[128,2048]{1,0:T(8,128)(2,1)}) custom-call(bf16[128,2048]{1,0:T(8,128)(2,1)} %get-tuple-element.4.mixed, bf16[128,2048]{1,0:T(8,128)(2,1)} %get-tuple-element.5.routed), custom_call_target="tpu_custom_call" | custom-call | tf_op jit(solution)/shard_map/hand_off/pallas_call | solution.py:950
